TPU v7x, 256 devices: a whole 4x4x8 slice. The times are simulated.
256 devices in a mesh: st: 16 (over y, x), tp: 16 (over z, core).
Axes of the slice: x: 4, y: 4, z: 8, core: 2. Of those that a mesh axis runs over, the one named last changes fastest.
Arguments:
- tokens: bfloat16 [8192, 4096], P('st', 'tp'), may hold values from -6 to 6
- w_query: bfloat16 [4096, 2048], P(None, 'tp'), may hold values from -0.09375 to 0.09375
- w_key: bfloat16 [4096, 2048], P(None, 'tp'), may hold values from -0.09375 to 0.09375
- w_value: bfloat16 [4096, 4096], P(None, 'tp'), may hold values from -0.09375 to 0.09375
- w_mem_query: bfloat16 [4096, 2048], P(None, 'tp'), may hold values from -0.09375 to 0.09375
- w_mem_key: bfloat16 [4096, 2048], P(None, 'tp'), may hold values from -0.09375 to 0.09375
- w_mem_value: bfloat16 [4096, 2048], P(None, 'tp'), may hold values from -0.09375 to 0.09375
- w_gate: bfloat16 [4096, 16], P(None, 'tp'), may hold values from -0.09375 to 0.09375
- w_lift: bfloat16 [16, 128, 256], P('tp'), may hold values from -4 to 4
- decay_rate: float32 [16], P('tp'), may hold values from 0.000390625 to 0.1
- store: bfloat16 [2048, 64, 4096], P('st', None, 'tp'), may hold values from -6 to 6
- passage_ids: int32 [64, 2], P('st'), may hold values from 0 to 2047, as said below
Outputs:
- mixed: bfloat16 [8192, 4096], P('st', 'tp')
Inputs may be any that keep to these rules, and one draw needn't show every extreme that they name: `passage_ids`: passage p is held by index p // 128 of st. Among the requests of the rows of one device along st, at most 1 name passages held by one index of st, and in every draw some index receives exactly 1 of them.
All inputs are finite; a program needn't handle non-finite values.
Results may differ from a plain program's by a relative error of at most 0.0095.
Values may be sent and summed in bfloat16 or wider, within the bound.
A program may use at most 64 MiB of HBM per device.

v0:
```python
import jax
import jax.numpy as jnp
from jax import lax
from jax.sharding import PartitionSpec as P

D = 4096
KEY_DIM = 128
VALUE_DIM = 256
MEM_DIM = 128
SEQ_LEN = 512
RET_BLOCK = 64
BLOCK = 128
PASS_ROWS = 64


norm_eps = 1e-06
rope_base = 10000.0


def rotate(values, positions):
    half_dim = values.shape[-1] // 2
    inverse = rope_base ** (-jnp.arange(half_dim, dtype=jnp.float32) / half_dim)
    angles = positions.astype(jnp.float32)[:, None] * inverse[None, :]
    cosine = jnp.cos(angles)[:, None, :]
    sine_table = jnp.sin(angles)[:, None, :]
    first_half = values[..., :half_dim]
    second_half = values[..., half_dim:]
    return jnp.concatenate(
        [
            first_half * cosine - second_half * sine_table,
            first_half * sine_table + second_half * cosine,
        ],
        axis=-1,
    )


def head_norm(values):
    return values * lax.rsqrt(jnp.mean(values * values, axis=-1, keepdims=True) + norm_eps)


def group_norm(values):
    centred = values - jnp.mean(values, axis=-1, keepdims=True)
    return centred * lax.rsqrt(jnp.mean(centred * centred, axis=-1, keepdims=True) + norm_eps)


def split_product(form, wide, narrow, wide_first):
    upper = wide.astype(jnp.bfloat16)
    lower = (wide - upper.astype(jnp.float32)).astype(jnp.bfloat16)
    if wide_first:
        return jnp.einsum(form, upper, narrow, preferred_element_type=jnp.float32) + jnp.einsum(
            form, lower, narrow, preferred_element_type=jnp.float32
        )
    return jnp.einsum(form, narrow, upper, preferred_element_type=jnp.float32) + jnp.einsum(
        form, narrow, lower, preferred_element_type=jnp.float32
    )


def retention(ret_query, ret_key, ret_value, rates, block_len):
    tokens_all, head_count, key_dim = ret_query.shape
    value_dim = ret_value.shape[-1]
    sequences = tokens_all // SEQ_LEN
    block_count = SEQ_LEN // block_len

    def blocked(array):
        shaped = array.reshape(sequences, block_count, block_len, head_count, array.shape[-1])
        return jnp.swapaxes(shaped, 0, 1)

    log_decay = -rates
    offsets = jnp.arange(block_len, dtype=jnp.float32)
    decay_query = jnp.exp(log_decay[None, :] * (offsets[:, None] + 1.0))
    distance = offsets[:, None] - offsets[None, :]
    decay_mask = jnp.where(
        distance[None] >= 0.0,
        jnp.exp(log_decay[:, None, None] * jnp.maximum(distance, 0.0)[None]),
        0.0,
    )
    decay_key = jnp.exp(log_decay[None, :] * (block_len - 1.0 - offsets[:, None]))
    decay_block = jnp.exp(log_decay * block_len)

    def advance(memory_state, pieces):
        query_block, key_block, value_block = pieces
        carried = (
            split_product("slhk,shkv->slhv", memory_state, query_block, False)
            * decay_query[None, :, :, None]
        )
        scores = (
            jnp.einsum(
                "slhk,smhk->shlm", query_block, key_block, preferred_element_type=jnp.float32
            )
            * decay_mask[None]
        )
        within = split_product("shlm,smhv->slhv", scores, value_block, True)
        weighted = key_block.astype(jnp.float32) * decay_key[None, :, :, None]
        memory_state = decay_block[None, :, None, None] * memory_state + split_product(
            "slhk,slhv->shkv", weighted, value_block, True
        )
        return (memory_state, carried + within)

    initial = jnp.zeros((sequences, head_count, key_dim, value_dim), jnp.float32)
    _, outputs = lax.scan(
        advance, initial, (blocked(ret_query), blocked(ret_key), blocked(ret_value))
    )
    return jnp.swapaxes(outputs, 0, 1).reshape(tokens_all, head_count, value_dim)


def per_device(
    tokens,
    w_query,
    w_key,
    w_value,
    w_mem_query,
    w_mem_key,
    w_mem_value,
    w_gate,
    w_lift,
    decay_rate,
    store,
    passage_ids,
):
    local_rows = tokens.shape[0]
    head_count = decay_rate.shape[0]
    projections = (w_query, w_key, w_value, w_mem_query, w_gate)
    shard_piece = lax.all_gather(tokens, "tp", axis=1, tiled=True)
    updated = tuple(
        (jnp.dot(shard_piece, weight, preferred_element_type=jnp.float32) for weight in projections)
    )
    widened = shard_piece.astype(jnp.float32)
    squares = jnp.sum(widened * widened, axis=1, keepdims=True)
    query_raw, key_raw, value_raw, mem_raw, gate_raw = updated
    row_scale = lax.rsqrt(squares / D + norm_eps)
    positions = jnp.arange(local_rows, dtype=jnp.int32) % SEQ_LEN
    ret_query = rotate(
        (query_raw * row_scale).reshape(local_rows, head_count, KEY_DIM), positions
    ).astype(jnp.bfloat16)
    ret_key = (
        rotate((key_raw * row_scale).reshape(local_rows, head_count, KEY_DIM), positions)
        * KEY_DIM ** (-0.5)
    ).astype(jnp.bfloat16)
    ret_value = (
        (value_raw * row_scale).astype(jnp.bfloat16).reshape(local_rows, head_count, VALUE_DIM)
    )
    mem_query = head_norm(mem_raw.reshape(local_rows, head_count, MEM_DIM)).astype(jnp.bfloat16)
    gate_value = jax.nn.sigmoid(gate_raw * row_scale)
    ret_norm = group_norm(retention(ret_query, ret_key, ret_value, decay_rate, RET_BLOCK))
    block_count, picks = passage_ids.shape
    request_count = block_count * picks
    group_count = lax.axis_size("st")
    capacity = max(1, 2 * request_count // group_count)
    held_count = store.shape[0]
    wanted = passage_ids.reshape(request_count)
    owners = wanted // held_count
    held_index = wanted % held_count
    ordinal = jnp.arange(request_count, dtype=jnp.int32)
    earlier = (owners[:, None] == owners[None, :]) & (ordinal[None, :] < ordinal[:, None])
    slot_index = jnp.sum(earlier.astype(jnp.int32), axis=1)
    placement = owners * capacity + slot_index
    selector = (
        placement[:, None] == jnp.arange(group_count * capacity, dtype=jnp.int32)[None, :]
    ).astype(jnp.int32)
    outgoing = jnp.sum(selector * held_index[:, None], axis=0).reshape(group_count, capacity)
    incoming = lax.all_to_all(outgoing, "st", split_axis=0, concat_axis=0, tiled=True)
    fetched = jnp.take(store, incoming.reshape(-1), axis=0)
    arrived = lax.all_to_all(
        fetched.reshape(incoming.shape + store.shape[1:]),
        "st",
        split_axis=0,
        concat_axis=0,
        tiled=True,
    )
    own_rows = arrived[owners, slot_index]
    shard_piece = lax.all_gather(own_rows, "tp", axis=2, tiled=True)
    key_sum = jnp.einsum("nrd,de->nre", shard_piece, w_mem_key, preferred_element_type=jnp.float32)
    value_sum = jnp.einsum(
        "nrd,de->nre", shard_piece, w_mem_value, preferred_element_type=jnp.float32
    )
    key_sum, value_sum = (key_sum, value_sum)
    leading = key_sum.shape[:2]
    key_rows = head_norm(key_sum.reshape(leading + (head_count, MEM_DIM))).astype(jnp.bfloat16)
    value_rows = value_sum.astype(jnp.bfloat16).reshape(leading + (head_count, MEM_DIM))
    query_blocks = mem_query.reshape(block_count, BLOCK, head_count, MEM_DIM)
    key_blocks = key_rows.reshape(block_count, picks * PASS_ROWS, head_count, MEM_DIM)
    value_blocks = value_rows.reshape(block_count, picks, PASS_ROWS, head_count, MEM_DIM)
    scores = jnp.einsum(
        "bthd,bkhd->bhtk", query_blocks, key_blocks, preferred_element_type=jnp.float32
    ) * MEM_DIM ** (-0.5)
    exponent = jnp.exp(scores).reshape(block_count, head_count, BLOCK, picks, PASS_ROWS)
    mass_sum = jnp.sum(exponent, axis=(3, 4))
    partial_value = jnp.einsum(
        "bhtpr,bprhd->bthpd",
        exponent.astype(jnp.bfloat16),
        value_blocks,
        preferred_element_type=jnp.float32,
    ).astype(jnp.bfloat16)
    summed = jnp.sum(partial_value.astype(jnp.float32), axis=3)
    mem_out = (
        (summed / jnp.swapaxes(mass_sum, 1, 2)[..., None])
        .astype(jnp.bfloat16)
        .reshape(local_rows, head_count, MEM_DIM)
    )
    mem_lift = jnp.einsum("thd,hde->the", mem_out, w_lift, preferred_element_type=jnp.float32)
    mixed = (ret_norm + gate_value[:, :, None] * mem_lift).astype(jnp.bfloat16)
    return mixed.reshape(local_rows, head_count * VALUE_DIM)


def solution(mesh):
    in_specs = (
        P("st", "tp"),
        P(None, "tp"),
        P(None, "tp"),
        P(None, "tp"),
        P(None, "tp"),
        P(None, "tp"),
        P(None, "tp"),
        P(None, "tp"),
        P("tp", None, None),
        P("tp"),
        P("st", None, "tp"),
        P("st", None),
    )
    out_specs = P("st", "tp")
    return jax.shard_map(
        per_device, mesh=mesh, in_specs=in_specs, out_specs=out_specs, check_vma=False
    )
```

profile of v0, /device:TPU:1, one launch (start us, length us, event | category | flops | bytes accessed | tf_op | source)
XLA Modules:
  0.0 126.2 jit_solution(3525777778997016366)
XLA Ops:
  6.5 0.7 all-gather.3.cloned.1.call-update
  7.3 0.8 copy.50
  8.5 13.8 %all_to_all.20 = s32[16,1,1]{2,1,0:T(1,128)S(1)} all-to-all(s32[16,1,1]{2,1,0:T(1,128)S(1)} %copy.51), channel_id=1, replica_groups=mesh['st'=16,'tp'=16] {'st'}, dimensions={0} | all-to-all | bytes 128 | tf_op jit(solution)/shard_map/all_to_all | solution.py:161
  22.7 2.9 %gather_fusion = bf16[16,64,256]{2,1,0:T(8,128)(2,1)S(1)} fusion(bf16[128,64,256]{2,1,0:T(8,128)(2,1)} %param.24, s32[1024]{0:T(1024)S(1)} %pad_clamp_fusion), kind=kCustom, calls=%fused_computation | custom fusion | bytes 1048640 | tf_op jit(solution)/shard_map/jit(_take)/gather | solution.py:162
  25.6 0.9 bitcast_select_fusion
  26.5 3.6 %all-to-all-start.1 = ((bf16[16,1,64,256]{3,2,1,0:T(8,128)(2,1)}), bf16[16,1,64,256]{3,2,1,0:T(8,128)(2,1)S(1)}, u32[]{:S(2)}, u32[]{:S(2)}) async-start(bf16[16,1,64,256]{3,2,1,0:T(8,128)(2,1)} %bitcast_select_fusion), calls=%async_computation.1 | async-start | bytes 1048576 | tf_op jit(solution)/shard_map/all_to_all | solution.py:163
  31.0 8.7 %all-to-all-done.1 = bf16[16,1,64,256]{3,2,1,0:T(8,128)(2,1)S(1)} async-done(((bf16[16,1,64,256]{3,2,1,0:T(8,128)(2,1)}), bf16[16,1,64,256]{3,2,1,0:T(8,128)(2,1)S(1)}, u32[]{:S(2)}, u32[]{:S(2)}) %all-to-all-start.1) | async-done | bytes 524320 | tf_op jit(solution)/shard_map/all_to_all | solution.py:163
  39.7 1.3 %gather_fusion.1 = bf16[8,64,256]{2,1,0:T(8,128)(2,1)} fusion(bf16[16,1,64,256]{3,2,1,0:T(8,128)(2,1)S(1)} %all-to-all-done.1, s32[8]{0:T(128)S(1)} %fusion.107), kind=kCustom, calls=%fused_computation.1 | custom fusion | bytes 524352 | tf_op jit(solution)/shard_map/gather | solution.py:170
  41.0 21.6 %all-gather.3.cloned.1.call-done = bf16[512,4096]{1,0:T(8,128)(2,1)} async-done(((bf16[512,256]{1,0:T(8,128)(2,1)}), bf16[512,4096]{1,0:T(8,128)(2,1)}) %all-gather.3.cloned.1.call-update) | async-done | bytes 4194320 | tf_op jit(solution)/shard_map/all_gather | solution.py:123
  62.6 3.2 %multiply_reduce_fusion = f32[512]{0:T(512)S(1)} fusion(bf16[512,4096]{1,0:T(8,128)(2,1)} %all-gather.3.cloned.1.call-done), kind=kLoop, calls=%fused_computation.71 | loop fusion | flops 6290944 | bytes 4196352 | tf_op jit(solution)/shard_map/reduce_sum | solution.py:128
  66.1 1.2 fusion.109
  67.3 1.5 %fusion.74 = f32[512,1,128]{0,2,1:T(8,128)S(1)} fusion(bf16[512,4096]{1,0:T(8,128)(2,1)S(1)} %copy-done.1, bf16[4096,128]{1,0:T(8,128)(2,1)S(1)} %copy-done.2, f32[512]{0:T(512)S(1)} %get-tuple-element.210), kind=kOutput, calls=%fused_computation.86 | convolution fusion | flops 536936448 | bytes 5507072 | tf_op jit(solution)/shard_map/dot_general | solution.py:125
  68.8 1.5 %fusion.75 = f32[512,1,128]{0,2,1:T(8,128)S(1)} fusion(bf16[512,4096]{1,0:T(8,128)(2,1)S(1)} %copy-done.1, bf16[4096,128]{1,0:T(8,128)(2,1)S(1)} %copy-done.3, f32[512]{0:T(512)S(1)} %get-tuple-element.210), kind=kOutput, calls=%fused_computation.88 | convolution fusion | flops 536936448 | bytes 5507072 | tf_op jit(solution)/shard_map/dot_general | solution.py:125
  70.3 0.6 fusion.91
  70.9 0.7 copy.56
  71.7 0.8 copy.57
  72.7 1.1 pad_maximum_fusion
  73.9 3.5 %fusion.69 = bf16[512,256]{1,0:T(8,128)(2,1)S(1)} fusion(bf16[512,4096]{1,0:T(8,128)(2,1)} %all-gather.3.cloned.1.call-done, bf16[4096,256]{1,0:T(8,128)(2,1)S(1)} %copy-done, f32[512]{0:T(512)S(1)} %get-tuple-element.210), kind=kOutput, calls=%fused_computation.78 | convolution fusion | flops 1074003968 | bytes 6555648 | tf_op jit(solution)/shard_map/dot_general | solution.py:125
  77.4 10.4 %while.15 = (s32[]{:T(128)}, f32[1,1,128,256]{3,2,1,0:T(8,128)S(1)}, f32[8,1,64,1,256]{4,2,3,1,0:T(8,128)S(1)}, f32[1]{0:T(128)}, bf16[8,1,64,1,128]{4,2,3,1,0:T...) while((s32[]{:T(128)}, ...), condition=%wide.region_2.3_spmd.clone.clone.clone, body=%wide.region_1.2_spmd.clone.clone.clone.sunk | while | flops 22532356 | bytes 1563791 | solution.py:100
  88.4 4.0 %multiply_reduce_fusion.3 = (f32[512]{0:T(512)S(1)}, f32[512,128]{1,0:T(8,128)S(1)}) fusion(bf16[512,4096]{1,0:T(8,128)(2,1)} %all-gather.3.cloned.1.call-done, bf16[4096,128]{1,0:T(8,128)(2,1)} %param.18), kind=kOutput, calls=%fused_computation.101 | convolution fusion | flops 537001472 | bytes 5507072 | tf_op jit(solution)/shard_map/dot_general | solution.py:125
  92.5 19.8 %all-gather.5.cloned.1.call-done = bf16[8,64,4096]{2,1,0:T(8,128)(2,1)} async-done(((bf16[8,64,256]{2,1,0:T(8,128)(2,1)}), bf16[8,64,4096]{2,1,0:T(8,128)(2,1)}) %all-gather.5.cloned.1.call-update) | async-done | bytes 4194320 | tf_op jit(solution)/shard_map/all_gather | solution.py:171
  112.3 4.0 %multiply_reduce_fusion.2 = (f32[8,64]{1,0:T(8,128)S(1)}, f32[8,64,128]{2,1,0:T(8,128)S(1)}) fusion(bf16[8,64,4096]{2,1,0:T(8,128)(2,1)} %all-gather.5.cloned.1.call-done, bf16[4096,128]{1,0:T(8,128)(2,1)} %param.19), kind=kOutput, calls=%fused_computation.99 | convolution fusion | flops 537001472 | bytes 5507072 | tf_op jit(solution)/shard_map/nrd,de->nre/dot_general | solution.py:172
  116.7 1.2 convolution_convert_fusion.1
  118.4 1.0 fusion.73
  (117 shorter events, 13.3 us)
Async XLA Ops:
  6.5 67.4 %copy-start = (bf16[4096,256]{1,0:T(8,128)(2,1)S(1)}, bf16[4096,256]{1,0:T(8,128)(2,1)}, u32[]{:S(2)}) copy-start(bf16[4096,256]{1,0:T(8,128)(2,1)} %param.17) | copy-start | bytes 6291460
  6.5 59.3 %copy-start.5 = (bf16[4096,1]{0,1:T(2,128)(2,1)S(1)}, bf16[4096,1]{0,1:T(2,128)(2,1)}, u32[]{:S(2)}) copy-start(bf16[4096,1]{0,1:T(2,128)(2,1)} %param.21) | copy-start | bytes 24580
  6.5 56.1 %all-gather.3.cloned.1.call-start = ((), (), s32[]{:S(2)}) async-start(), calls=%async_computation.2 | async-start | bytes 4456448 | tf_op jit(solution)/shard_map/all_gather | solution.py:123
  26.5 13.2 %all-to-all-start.1 = ((bf16[16,1,64,256]{3,2,1,0:T(8,128)(2,1)}), bf16[16,1,64,256]{3,2,1,0:T(8,128)(2,1)S(1)}, u32[]{:S(2)}, u32[]{:S(2)}) async-start(bf16[16,1,64,256]{3,2,1,0:T(8,128)(2,1)} %bitcast_select_fusion), calls=%async_computation.1 | async-start | bytes 1048576 | tf_op jit(solution)/shard_map/all_to_all | solution.py:163
  30.1 82.2 %all-gather.5.cloned.1.call-start = ((), (), s32[]{:S(2)}) async-start(), calls=%async_computation.3 | async-start | bytes 4456448 | tf_op jit(solution)/shard_map/all_gather | solution.py:171
  62.6 3.4 %copy-start.1 = (bf16[512,4096]{1,0:T(8,128)(2,1)S(1)}, bf16[512,4096]{1,0:T(8,128)(2,1)}, u32[]{:S(2)}) copy-start(bf16[512,4096]{1,0:T(8,128)(2,1)} %all-gather.3.cloned.1.call-done) | copy-start | bytes 12582916
  62.6 4.7 %copy-start.2 = (bf16[4096,128]{1,0:T(8,128)(2,1)S(1)}, bf16[4096,128]{1,0:T(8,128)(2,1)}, u32[]{:S(2)}) copy-start(bf16[4096,128]{1,0:T(8,128)(2,1)} %param.15) | copy-start | bytes 3145732
  67.2 1.6 %copy-start.3 = (bf16[4096,128]{1,0:T(8,128)(2,1)S(1)}, bf16[4096,128]{1,0:T(8,128)(2,1)}, u32[]{:S(2)}) copy-start(bf16[4096,128]{1,0:T(8,128)(2,1)} %param.16) | copy-start | bytes 3145732
  112.3 4.4 %copy-start.6 = (bf16[8,64,4096]{2,1,0:T(8,128)(2,1)S(1)}, bf16[8,64,4096]{2,1,0:T(8,128)(2,1)}, u32[]{:S(2)}) copy-start(bf16[8,64,4096]{2,1,0:T(8,128)(2,1)} %all-gather.5.cloned.1.call-done) | copy-start | bytes 12582916
  112.3 4.4 %copy-start.7 = (bf16[4096,128]{1,0:T(8,128)(2,1)S(1)}, bf16[4096,128]{1,0:T(8,128)(2,1)}, u32[]{:S(2)}) copy-start(bf16[4096,128]{1,0:T(8,128)(2,1)} %param.20) | copy-start | bytes 3145732
  116.6 1.7 %copy-start.4 = (bf16[1,128,256]{2,1,0:T(8,128)(2,1)S(1)}, bf16[1,128,256]{2,1,0:T(8,128)(2,1)}, u32[]{:S(2)}) copy-start(bf16[1,128,256]{2,1,0:T(8,128)(2,1)} %param.22) | copy-start | bytes 196612
Sparse Core Ops, SparseCore 0:
  9.1 53.4 all-gather.2
  64.4 47.8 all-gather.4
where the time goes:
time: 127 us; the launch traced here: 126 us
  waiting for transfers between devices  50.8 us (40%)
  matrix products  28.3 us (22%)
  between operations  14.4 us (11%)
  blocking collectives  13.8 us (11%)
  other arithmetic  7.54 us (6%)
  local copies, waits for them, and re-layouts  7.44 us (6%)
  starting transfers between devices  3.61 us (3%)
    all_gather x1, waiting for transfers between devices, per_device(): shard_piece = lax.all_gather(tokens, 'tp', axis=1, tiled=True)  21.6 us
    all_gather x1, waiting for transfers between devices, per_device(): shard_piece = lax.all_gather(own_rows, 'tp', axis=2, tiled=True)  19.8 us
    all_to_all x1, blocking collectives, per_device(): lax.all_to_all(outgoing, 'st', split_axis=0, concat_axis=0, tiled=True)  13.8 us
    dot_general x5, matrix products, per_device(): jnp.dot(shard_piece, weight, preferred_element_type=jnp.float32)  11.6 us
    all_to_all x1, waiting for transfers between devices, per_device(): lax.all_to_all(fetched.reshape(incoming.shape + store.shape[1:]), 'st', s...  8.74 us
    dot_general x1, matrix products, per_device(): jnp.einsum('nrd,de->nre', shard_piece, w_mem_key, preferred_element_type=...  3.96 us
    all_to_all x1, starting transfers between devices, per_device(): lax.all_to_all(fetched.reshape(incoming.shape + store.shape[1:]), 'st', s...  3.57 us
    dot_general x16, matrix products, split_product(): jnp.einsum(form, lower, narrow, preferred_element_type=jnp.float32)  3.29 us
  transfers between devices with their start and end apart: 3, of which 3 were waited for; matrix products, arithmetic and copies ran while one was open for 29% of the time, Pallas kernels for 0%

commit v1 on v0

v1 whole, which is shorter than its diff:
```python
import jax
import jax.numpy as jnp
import numpy as np
from jax import lax
from jax.experimental import pallas as pl
from jax.experimental.pallas import tpu as pltpu
from jax.sharding import PartitionSpec as P

D = 4096
KEY_DIM = 128
VALUE_DIM = 256
MEM_DIM = 128
SEQ_LEN = 512
BLOCK = 128
PICKS = 2
PASS_ROWS = 64
PASS_SHIFT = 7
N_ST = 16
RING = 8
BLOCKS = 4
SLOTS = 14
HALF = 256
TOK_COLS = 640

norm_eps = 1e-06
rope_base = 10000.0

F32 = jnp.float32
BF16 = jnp.bfloat16
MESH = pl.DeviceIdType.MESH


def rotary_tables():
    half = KEY_DIM // 2
    inverse = rope_base ** (-np.arange(half, dtype=np.float64) / half)
    angles = np.arange(SEQ_LEN, dtype=np.float64)[:, None] * inverse[None, :]
    cosine, sine = np.cos(angles), np.sin(angles)
    cos_table = np.concatenate([cosine, cosine], axis=1).astype(np.float32)
    sin_table = np.concatenate([-sine, sine], axis=1).astype(np.float32)
    return cos_table, sin_table


def dot(a, b):
    return jnp.dot(a, b, preferred_element_type=F32)


def dot_t(a, b):
    return lax.dot_general(a, b, (((1,), (1,)), ((), ())), preferred_element_type=F32)


def kernel(
    tok,
    wq,
    wk,
    wv,
    wmq,
    wmk,
    wmv,
    wg,
    wl,
    store,
    cos_in,
    sin_in,
    decay,
    ids,
    out,
    x,
    wt,
    wm,
    store_v,
    outbox,
    inbox,
    acc,
    squares,
    gates,
    acc_p,
    key_v,
    value_v,
    mem_q,
    gate_v,
    ret_norm,
    wg_v,
    wg_f,
    wl_v,
    cos_v,
    sin_v,
    out_v,
    ids_all,
    tok_sem,
    local_sem,
    out_sem,
    z_send,
    z_recv,
    d_send,
    d_recv,
    i_send,
    i_recv,
    s_send,
    s_recv,
):
    st = lax.axis_index("st")
    tp = lax.axis_index("tp")
    z = lax.div(tp, 2)
    core = lax.rem(tp, 2)
    other = 1 - core
    up = lax.rem(z + 1, RING) * 2 + core
    down = lax.rem(z + RING - 1, RING) * 2 + core
    partner = z * 2 + other

    def peer(offset):
        return lax.rem(st + offset, N_ST)

    tok_copies = [
        pltpu.make_async_copy(
            tok.at[pl.ds(b * BLOCK, BLOCK), :], x.at[0, z, b, core], tok_sem.at[b]
        )
        for b in range(BLOCKS)
    ]
    for copy in tok_copies:
        copy.start()
    local = [
        (wg, wg_v),
        (wq, wt.at[:, pl.ds(0, 128)]),
        (wk, wt.at[:, pl.ds(128, 128)]),
        (wv, wt.at[:, pl.ds(256, 256)]),
        (wmq, wt.at[:, pl.ds(512, 128)]),
        (store, store_v),
        (wmk, wm.at[:, pl.ds(0, 128)]),
        (wmv, wm.at[:, pl.ds(128, 128)]),
        (wl, wl_v),
        (cos_in, cos_v),
        (sin_in, sin_v),
    ]
    local_copies = [
        pltpu.make_async_copy(src, dst, local_sem.at[i]) for i, (src, dst) in enumerate(local)
    ]
    for copy in local_copies:
        copy.start()

    barrier = pltpu.get_barrier_semaphore()
    for target in (up, down, partner):
        pl.semaphore_signal(barrier, inc=1, device_id={"tp": target}, device_id_type=MESH)

    @pl.loop(1, N_ST)
    def _(offset):
        pl.semaphore_signal(
            barrier, inc=1, device_id={"st": peer(offset)}, device_id_type=MESH
        )

    pl.semaphore_wait(barrier, 3 + N_ST - 1)

    def slot_block(d, s):
        return lax.rem(s + 2 * d, BLOCKS)

    def chunk_at(d, hops):
        return lax.rem(z + RING - hops, RING) if d == 0 else lax.rem(z + hops, RING)

    def z_copy(phase, d, s):
        ref = x.at[phase, chunk_at(d, lax.div(s, BLOCKS)), slot_block(d, s), core]
        return pltpu.make_async_remote_copy(
            src_ref=ref,
            dst_ref=ref,
            send_sem=z_send.at[phase, d, s],
            recv_sem=z_recv.at[phase, d, s],
            device_id={"tp": up if d == 0 else down},
            device_id_type=MESH,
        )

    def z_arrival(phase, d, s):
        ref = x.at[phase, chunk_at(d, lax.div(s, BLOCKS) + 1), slot_block(d, s), core]
        return pltpu.make_async_remote_copy(
            src_ref=ref,
            dst_ref=ref,
            send_sem=z_send.at[phase, d, s],
            recv_sem=z_recv.at[phase, d, s],
            device_id={"tp": up if d == 0 else down},
            device_id_type=MESH,
        )

    def d_copy(phase, index, chunk, b, half):
        ref = x.at[phase, chunk, b, half]
        return pltpu.make_async_remote_copy(
            src_ref=ref,
            dst_ref=ref,
            send_sem=d_send.at[phase, index],
            recv_sem=d_recv.at[phase, index],
            device_id={"tp": partner},
            device_id_type=MESH,
        )

    def d_slot(d, s):
        return BLOCKS + d * SLOTS + s

    def send_own(phase):
        for b in range(BLOCKS):
            z_copy(phase, 0, jnp.int32(b)).start()
            z_copy(phase, 1, jnp.int32(b)).start()
        for b in range(BLOCKS):
            d_copy(phase, b, z, b, core).start()

    for copy in tok_copies:
        copy.wait()
    send_own(0)

    def id_copy(offset):
        return pltpu.make_async_remote_copy(
            src_ref=ids,
            dst_ref=ids_all.at[st],
            send_sem=i_send.at[offset],
            recv_sem=i_recv.at[offset],
            device_id={"st": peer(offset)},
            device_id_type=MESH,
        )

    @pl.loop(1, N_ST)
    def _(offset):
        id_copy(offset).start()

    local_copies[0].wait()
    for chunk in range(RING):
        wg_f[chunk] = wg_v[:, chunk * 512 : (chunk + 1) * 512].astype(F32)
    for copy in local_copies[1:]:
        copy.wait()

    def add_tokens(chunk, b, first=False):
        both = jnp.concatenate([x[0, chunk, b, 0], x[0, chunk, b, 1]], axis=1)
        rows = pl.ds(pl.multiple_of(chunk * 512, 512), 512)
        product = dot(both, wt[rows, :])
        wide = both.astype(F32)
        square = wide * wide
        gated = wide * wg_f[chunk]
        square = (square[:, 0:128] + square[:, 128:256]) + (
            square[:, 256:384] + square[:, 384:512]
        )
        gated = (gated[:, 0:128] + gated[:, 128:256]) + (gated[:, 256:384] + gated[:, 384:512])
        if first:
            acc[b] = product
            squares[b] = square
            gates[b] = gated
        else:
            acc[b] += product
            squares[b] += square
            gates[b] += gated

    def add_passages(chunk, b, first=False):
        both = jnp.concatenate([x[1, chunk, b, 0], x[1, chunk, b, 1]], axis=1)
        rows = pl.ds(pl.multiple_of(chunk * 512, 512), 512)
        product = dot(both, wm[rows, :])
        if first:
            acc_p[b] = product
        else:
            acc_p[b] += product

    def take_slot(phase, s, relay):
        for d in range(2):
            z_arrival(phase, d, s).wait_recv()
            if relay is True:
                z_copy(phase, d, s + BLOCKS).start()
            elif relay is not False:

                @pl.when(relay)
                def _():
                    z_copy(phase, d, s + BLOCKS).start()

            chunk = chunk_at(d, lax.div(s, BLOCKS) + 1)
            d_copy(phase, d_slot(d, s), chunk, slot_block(d, s), core).start()

    def add_slot(phase, s):
        for d in range(2):
            chunk = chunk_at(d, lax.div(s, BLOCKS) + 1)
            b = slot_block(d, s)
            d_copy(phase, d_slot(d, s), chunk, b, other).wait_recv()
            if phase == 0:
                add_tokens(chunk, b)
            else:
                add_passages(chunk, b)

    for b in range(BLOCKS):
        d_copy(0, b, z, b, other).wait_recv()
        add_tokens(z, b, first=True)

    def id_arrival(offset):
        return pltpu.make_async_remote_copy(
            src_ref=ids,
            dst_ref=ids_all.at[peer(N_ST - offset)],
            send_sem=i_send.at[offset],
            recv_sem=i_recv.at[offset],
            device_id={"st": peer(offset)},
            device_id_type=MESH,
        )

    take_slot(0, jnp.int32(0), True)

    @pl.loop(1, N_ST)
    def _(offset):
        id_arrival(offset).wait_recv()

    def wanted_row(read):
        row = jnp.int32(0)
        for pick in range(PICKS):
            for b in range(BLOCKS):
                ident = read(pick, b)
                mine = lax.shift_right_logical(ident, PASS_SHIFT) == st
                row = row + jnp.where(mine, ident & ((1 << PASS_SHIFT) - 1), 0)
        return row

    inbox[st] = store_v[wanted_row(lambda pick, b: ids[pick, b])]

    @pl.loop(1, N_ST)
    def _(offset):
        target = peer(offset)
        outbox[offset] = store_v[wanted_row(lambda pick, b: ids_all[target, pick, b])]

    take_slot(0, jnp.int32(1), True)
    add_slot(0, jnp.int32(0))

    def row_copy(offset, place):
        return pltpu.make_async_remote_copy(
            src_ref=outbox.at[offset],
            dst_ref=inbox.at[place],
            send_sem=s_send.at[offset],
            recv_sem=s_recv.at[offset],
            device_id={"st": peer(offset)},
            device_id_type=MESH,
        )

    @pl.loop(1, N_ST)
    def _(offset):
        row_copy(offset, st).start()

    @pl.loop(2, 9)
    def _(s):
        take_slot(0, s, True)
        add_slot(0, s - 1)

    @pl.loop(1, N_ST)
    def _(offset):
        row_copy(offset, peer(N_ST - offset)).wait_recv()

    for b in range(BLOCKS):
        for pick in range(PICKS):
            owner = lax.shift_right_logical(ids[pick, b], PASS_SHIFT)
            x[1, z, b, core, pick * PASS_ROWS : (pick + 1) * PASS_ROWS, :] = inbox[owner]

    take_slot(0, jnp.int32(9), True)
    add_slot(0, jnp.int32(8))
    send_own(1)

    @pl.loop(10, SLOTS)
    def _(s):
        take_slot(0, s, False)
        add_slot(0, s - 1)

    rate = decay[0]

    def finish_tokens(b):
        mean_square = jnp.sum(squares[b], axis=1, keepdims=True) * (1.0 / D)
        scale = lax.rsqrt(mean_square + norm_eps)
        cosine = cos_v[b * BLOCK : (b + 1) * BLOCK, :]
        sine = sin_v[b * BLOCK : (b + 1) * BLOCK, :]

        def rotate(values):
            return values * cosine + pltpu.roll(values, KEY_DIM // 2, 1) * sine

        query = rotate(acc[b, :, 0:128] * scale).astype(BF16)
        key = (rotate(acc[b, :, 128:256] * scale) * KEY_DIM ** (-0.5)).astype(BF16)
        key_v[b * BLOCK : (b + 1) * BLOCK, :] = key
        value_v[b * BLOCK : (b + 1) * BLOCK, :] = (acc[b, :, 256:512] * scale).astype(BF16)
        memory = acc[b, :, 512:640]
        mean = jnp.mean(memory * memory, axis=1, keepdims=True)
        mem_q[b] = (memory * lax.rsqrt(mean + norm_eps)).astype(BF16)
        gate = jnp.sum(gates[b], axis=1, keepdims=True) * scale
        gate_v[b] = jnp.broadcast_to(jax.nn.sigmoid(gate), (BLOCK, 128))

        span = (b + 1) * BLOCK
        keys = key_v[0:span, :]
        values = value_v[0:span, :]
        row = lax.broadcasted_iota(jnp.int32, (BLOCK, span), 0) + b * BLOCK
        column = lax.broadcasted_iota(jnp.int32, (BLOCK, span), 1)
        distance = (row - column).astype(F32)
        mask = jnp.where(distance >= 0.0, jnp.exp(-rate * jnp.maximum(distance, 0.0)), 0.0)
        scores = dot_t(query, keys) * mask
        upper = scores.astype(BF16)
        lower = (scores - upper.astype(F32)).astype(BF16)
        mixed = dot(upper, values) + dot(lower, values)
        centred = mixed - jnp.mean(mixed, axis=1, keepdims=True)
        variance = jnp.mean(centred * centred, axis=1, keepdims=True)
        ret_norm[b] = centred * lax.rsqrt(variance + norm_eps)

    def out_copy(b):
        return pltpu.make_async_copy(
            out_v.at[b], out.at[pl.ds(b * BLOCK, BLOCK), :], out_sem.at[b]
        )

    def finish_block(b):
        raw = acc_p[b, :, 0:128]
        mean = jnp.mean(raw * raw, axis=1, keepdims=True)
        pass_key = (raw * lax.rsqrt(mean + norm_eps)).astype(BF16)
        pass_value = acc_p[b, :, 128:256].astype(BF16)
        exponent = jnp.exp(dot_t(mem_q[b], pass_key) * MEM_DIM ** (-0.5))
        mass = jnp.sum(exponent, axis=1, keepdims=True)
        summed = dot(exponent.astype(BF16), pass_value)
        mem_out = (summed / mass).astype(BF16)
        lift = dot(mem_out, wl_v[0])
        gate = gate_v[b]
        gate = jnp.concatenate([gate, gate], axis=1)
        out_v[b] = (ret_norm[b] + gate * lift).astype(BF16)
        out_copy(b).start()

    for s in range(SLOTS):
        take_slot(1, jnp.int32(s), s < SLOTS - BLOCKS)
        if s == 0:
            add_slot(0, jnp.int32(SLOTS - 1))
            for b in range(BLOCKS):
                d_copy(1, b, z, b, other).wait_recv()
                add_passages(z, b, first=True)
        else:
            add_slot(1, jnp.int32(s - 1))
        if s < BLOCKS:
            finish_tokens(s)
        if s == 8:

            @pl.loop(0, SLOTS)
            def _(n):
                z_copy(0, 0, n).wait_send()
                z_copy(0, 1, n).wait_send()

            @pl.loop(0, BLOCKS + 2 * SLOTS)
            def _(n):
                d_copy(0, n, z, 0, core).wait_send()

            @pl.loop(1, N_ST)
            def _(offset):
                id_copy(offset).wait_send()
                row_copy(offset, st).wait_send()

    finish_block(0)
    finish_block(2)
    add_slot(1, jnp.int32(SLOTS - 1))
    finish_block(1)
    finish_block(3)

    @pl.loop(0, SLOTS)
    def _(n):
        z_copy(1, 0, n).wait_send()
        z_copy(1, 1, n).wait_send()

    @pl.loop(0, BLOCKS + 2 * SLOTS)
    def _(n):
        d_copy(1, n, z, 0, core).wait_send()

    for b in range(BLOCKS):
        out_copy(b).wait()


def per_device(
    tokens,
    w_query,
    w_key,
    w_value,
    w_mem_query,
    w_mem_key,
    w_mem_value,
    w_gate,
    w_lift,
    decay_rate,
    store,
    passage_ids,
):
    cos_table, sin_table = rotary_tables()
    hbm = pl.BlockSpec(memory_space=pl.ANY)
    smem = pl.BlockSpec(memory_space=pltpu.SMEM)
    dma = pltpu.SemaphoreType.DMA
    return pl.pallas_call(
        kernel,
        out_shape=jax.ShapeDtypeStruct((SEQ_LEN, VALUE_DIM), BF16),
        in_specs=[hbm] * 12 + [smem] * 2,
        out_specs=hbm,
        scratch_shapes=[
            pltpu.VMEM((2, RING, BLOCKS, 2, BLOCK, HALF), BF16),
            pltpu.VMEM((D, TOK_COLS), BF16),
            pltpu.VMEM((D, 2 * MEM_DIM), BF16),
            pltpu.VMEM(store.shape, BF16),
            pltpu.VMEM((N_ST, PASS_ROWS, HALF), BF16),
            pltpu.VMEM((N_ST, PASS_ROWS, HALF), BF16),
            pltpu.VMEM((BLOCKS, BLOCK, TOK_COLS), F32),
            pltpu.VMEM((BLOCKS, BLOCK, 128), F32),
            pltpu.VMEM((BLOCKS, BLOCK, 128), F32),
            pltpu.VMEM((BLOCKS, BLOCK, 2 * MEM_DIM), F32),
            pltpu.VMEM((SEQ_LEN, KEY_DIM), BF16),
            pltpu.VMEM((SEQ_LEN, VALUE_DIM), BF16),
            pltpu.VMEM((BLOCKS, BLOCK, MEM_DIM), BF16),
            pltpu.VMEM((BLOCKS, BLOCK, 128), F32),
            pltpu.VMEM((BLOCKS, BLOCK, VALUE_DIM), F32),
            pltpu.VMEM((1, D), BF16),
            pltpu.VMEM((RING, 1, 512), F32),
            pltpu.VMEM((1, MEM_DIM, VALUE_DIM), BF16),
            pltpu.VMEM((SEQ_LEN, KEY_DIM), F32),
            pltpu.VMEM((SEQ_LEN, KEY_DIM), F32),
            pltpu.VMEM((BLOCKS, BLOCK, VALUE_DIM), BF16),
            pltpu.SMEM((N_ST, PICKS, BLOCKS), jnp.int32),
            dma((BLOCKS,)),
            dma((11,)),
            dma((BLOCKS,)),
            dma((2, 2, SLOTS)),
            dma((2, 2, SLOTS)),
            dma((2, BLOCKS + 2 * SLOTS)),
            dma((2, BLOCKS + 2 * SLOTS)),
            dma((N_ST,)),
            dma((N_ST,)),
            dma((N_ST,)),
            dma((N_ST,)),
        ],
        compiler_params=pltpu.CompilerParams(
            collective_id=0, has_side_effects=True, vmem_limit_bytes=48 * 1024 * 1024
        ),
        name="fused_layer",
    )(
        tokens,
        w_query,
        w_key,
        w_value,
        w_mem_query,
        w_mem_key,
        w_mem_value,
        w_gate.reshape(1, D),
        w_lift,
        store,
        cos_table,
        sin_table,
        decay_rate,
        passage_ids.T,
    )


def solution(mesh):
    in_specs = (
        P("st", "tp"),
        P(None, "tp"),
        P(None, "tp"),
        P(None, "tp"),
        P(None, "tp"),
        P(None, "tp"),
        P(None, "tp"),
        P(None, "tp"),
        P("tp", None, None),
        P("tp"),
        P("st", None, "tp"),
        P("st", None),
    )
    out_specs = P("st", "tp")
    return jax.shard_map(
        per_device, mesh=mesh, in_specs=in_specs, out_specs=out_specs, check_vma=False
    )
```

time: 127 us -> 72.6 us (0.57)
  Pallas kernels: 0 us -> 60.8 us
  waiting for transfers between devices: 50.8 us -> 0 us
  matrix products: 28.3 us -> 0 us
  blocking collectives: 13.8 us -> 0 us
  between operations: 14.4 us -> 0.68 us
  other arithmetic: 7.54 us -> 0 us
  starting transfers between devices: 3.61 us -> 0 us
  local copies, waits for them, and re-layouts: 7.44 us -> 10.7 us
    pallas_call x0 -> x1, Pallas kernels: none -> 60.8 us  [per_device(): pl.pallas_call(kernel, out_shape=jax.ShapeDtypeStruct((SEQ_LEN, VALUE_DIM...]
    all_gather x2 -> x0, waiting for transfers between devices: 41.4 us -> none  [the longest x1 21.6 us: per_device(): shard_piece = lax.all_gather(tokens, 'tp', axis=1, tiled=True)]
    dot_general x66 -> x0, matrix products: 28.3 us -> none  [the longest x5 11.6 us: per_device(): jnp.dot(shard_piece, weight, preferred_element_type=jnp.float32)]
    all_to_all x1 -> x0, blocking collectives: 13.8 us -> none  [per_device(): lax.all_to_all(outgoing, 'st', split_axis=0, concat_axis=0, tiled=True)]
    unnamed x17 -> x21, local copies, waits for them, and re-layouts: 1.01 us -> 10.7 us
    all_to_all x1 -> x0, waiting for transfers between devices: 8.74 us -> none  [per_device(): lax.all_to_all(fetched.reshape(incoming.shape + store.shape[1:]), 'st', s...]
    gather x2 -> x0, local copies, waits for them, and re-layouts: 4.16 us -> none  [the longest x1 2.89 us: per_device(): fetched = jnp.take(store, incoming.reshape(-1), axis=0)]
    reduce_sum x5 -> x0, other arithmetic: 3.91 us -> none  [the longest x1 3.23 us: per_device(): squares = jnp.sum(widened * widened, axis=1, keepdims=True)]
  transfers between devices with their start and end apart: 3 -> 0, of which waited for: 3 -> 0; matrix products, arithmetic and copies ran while one was open for 29% -> 0% of each run, Pallas kernels for 0% -> 0%
where the time goes in v1:
time: 72.6 us; the launch traced here: 72.1 us
  Pallas kernels  60.8 us (84%)
  local copies, waits for them, and re-layouts  10.7 us (15%)
    pallas_call x1, Pallas kernels, per_device(): pl.pallas_call(kernel, out_shape=jax.ShapeDtypeStruct((SEQ_LEN, VALUE_DIM...  60.8 us
    unnamed x21, local copies, waits for them, and re-layouts  10.7 us

profile of v1, /device:TPU:1, one launch (start us, length us, event | category | flops | bytes accessed | tf_op | source)
XLA Modules:
  0.0 72.1 jit_solution(8569545245667373863)
XLA Ops:
  0.7 0.0 copy-start
  0.7 1.2 %copy-done = bf16[4096,128]{1,0:T(8,128)(2,1)S(1)} copy-done((bf16[4096,128]{1,0:T(8,128)(2,1)S(1)}, bf16[4096,128]{1,0:T(8,128)(2,1)}, u32[]{:S(2)}) %copy-start) | copy-done | bytes 1048600
  1.9 0.0 copy-start.1
  1.9 1.2 %copy-done.1 = bf16[4096,128]{1,0:T(8,128)(2,1)S(1)} copy-done((bf16[4096,128]{1,0:T(8,128)(2,1)S(1)}, bf16[4096,128]{1,0:T(8,128)(2,1)}, u32[]{:S(2)}) %copy-start.1) | copy-done | bytes 1048600
  3.1 0.0 copy-start.2
  3.1 1.2 %copy-done.2 = bf16[4096,128]{1,0:T(8,128)(2,1)S(1)} copy-done((bf16[4096,128]{1,0:T(8,128)(2,1)S(1)}, bf16[4096,128]{1,0:T(8,128)(2,1)}, u32[]{:S(2)}) %copy-start.2) | copy-done | bytes 1048600
  4.3 0.0 copy-start.3
  4.3 1.2 %copy-done.3 = bf16[4096,128]{1,0:T(8,128)(2,1)S(1)} copy-done((bf16[4096,128]{1,0:T(8,128)(2,1)S(1)}, bf16[4096,128]{1,0:T(8,128)(2,1)}, u32[]{:S(2)}) %copy-start.3) | copy-done | bytes 1048600
  5.6 0.0 copy-start.4
  5.6 0.9 %copy-done.4 = bf16[512,256]{1,0:T(8,128)(2,1)S(1)} copy-done((bf16[512,256]{1,0:T(8,128)(2,1)S(1)}, bf16[512,256]{1,0:T(8,128)(2,1)}, u32[]{:S(2)}) %copy-start.4) | copy-done | bytes 262168
  6.5 0.0 copy-start.5
  6.5 0.9 %copy-done.5 = f32[512,128]{1,0:T(8,128)S(1)} copy-done((f32[512,128]{1,0:T(8,128)S(1)}, f32[512,128]{1,0:T(8,128)}, u32[]{:S(2)}) %copy-start.5) | copy-done | bytes 262168
  7.5 0.0 copy-start.6
  7.5 0.9 %copy-done.6 = f32[512,128]{1,0:T(8,128)S(1)} copy-done((f32[512,128]{1,0:T(8,128)S(1)}, f32[512,128]{1,0:T(8,128)}, u32[]{:S(2)}) %copy-start.6) | copy-done | bytes 262168
  8.4 0.0 copy-start.7
  8.4 0.8 %copy-done.7 = bf16[1,128,256]{2,1,0:T(8,128)(2,1)S(1)} copy-done((bf16[1,128,256]{2,1,0:T(8,128)(2,1)S(1)}, bf16[1,128,256]{2,1,0:T(8,128)(2,1)}, u32[]{:S(2)}) %copy-start.7) | copy-done | bytes 65560
  9.2 0.0 copy-start.8
  9.2 0.7 copy-done.8
  10.0 0.0 copy-start.9
  10.0 0.7 copy-done.9
  10.6 60.8 %fused_layer.1 = bf16[512,256]{1,0:T(8,128)(2,1)S(1)} custom-call(bf16[512,256]{1,0:T(8,128)(2,1)S(1)} %copy-done.4, bf16[4096,128]{1,0:T(8,128)(2,1)S(1)} %copy-done, bf16[4096,128]{1,0:T(8,128)(2,1)S(1)} %copy-done.1, bf16[4096,256]{1,0:T(8,128)(2,1)} %wv.1, bf16[4096,128]{1,0:T(8,128)(2,1)S(1)} %copy-done.2, bf16[4096,128]{1,0:T(8,128)(2,1)S(1)} %copy-done.3, ...), custom_call_target="tpu_custom_call" | custom-call | tf_op jit(solution)/shard_map/fused_layer/pallas_call | solution.py:474
  71.4 0.7 copy.17
Async XLA Ops:
  0.7 1.2 %copy-start = (bf16[4096,128]{1,0:T(8,128)(2,1)S(1)}, bf16[4096,128]{1,0:T(8,128)(2,1)}, u32[]{:S(2)}) copy-start(bf16[4096,128]{1,0:T(8,128)(2,1)} %wq.1) | copy-start | bytes 3145732
  1.9 1.2 %copy-start.1 = (bf16[4096,128]{1,0:T(8,128)(2,1)S(1)}, bf16[4096,128]{1,0:T(8,128)(2,1)}, u32[]{:S(2)}) copy-start(bf16[4096,128]{1,0:T(8,128)(2,1)} %wk.1) | copy-start | bytes 3145732
  3.1 1.2 %copy-start.2 = (bf16[4096,128]{1,0:T(8,128)(2,1)S(1)}, bf16[4096,128]{1,0:T(8,128)(2,1)}, u32[]{:S(2)}) copy-start(bf16[4096,128]{1,0:T(8,128)(2,1)} %wmq.1) | copy-start | bytes 3145732
  4.3 1.2 %copy-start.3 = (bf16[4096,128]{1,0:T(8,128)(2,1)S(1)}, bf16[4096,128]{1,0:T(8,128)(2,1)}, u32[]{:S(2)}) copy-start(bf16[4096,128]{1,0:T(8,128)(2,1)} %wmk.1) | copy-start | bytes 3145732
  5.6 0.9 %copy-start.4 = (bf16[512,256]{1,0:T(8,128)(2,1)S(1)}, bf16[512,256]{1,0:T(8,128)(2,1)}, u32[]{:S(2)}) copy-start(bf16[512,256]{1,0:T(8,128)(2,1)} %tok.1) | copy-start | bytes 786436
  6.5 0.9 %copy-start.5 = (f32[512,128]{1,0:T(8,128)S(1)}, f32[512,128]{1,0:T(8,128)}, u32[]{:S(2)}) copy-start(f32[512,128]{1,0:T(8,128)} %constant.5.clone.sin_in) | copy-start | bytes 786436
  7.5 0.9 %copy-start.6 = (f32[512,128]{1,0:T(8,128)S(1)}, f32[512,128]{1,0:T(8,128)}, u32[]{:S(2)}) copy-start(f32[512,128]{1,0:T(8,128)} %constant.4.clone.cos_in) | copy-start | bytes 786436
  8.4 0.8 %copy-start.7 = (bf16[1,128,256]{2,1,0:T(8,128)(2,1)S(1)}, bf16[1,128,256]{2,1,0:T(8,128)(2,1)}, u32[]{:S(2)}) copy-start(bf16[1,128,256]{2,1,0:T(8,128)(2,1)} %wl.1) | copy-start | bytes 196612
  9.2 0.7 copy-start.8
  10.0 0.7 copy-start.9

commit v2 on v1

--- a/solution.py
+++ b/solution.py
@@ -512,7 +512,7 @@
             dma((N_ST,)),
         ],
         compiler_params=pltpu.CompilerParams(
-            collective_id=0, has_side_effects=True, vmem_limit_bytes=48 * 1024 * 1024
+            collective_id=0, has_side_effects=True, vmem_limit_bytes=67043328
         ),
         name="fused_layer",
     )(

time: 72.6 us -> 61.6 us (0.85)
  local copies, waits for them, and re-layouts: 10.7 us -> 1.67 us
  Pallas kernels: 60.8 us -> 59.2 us
    unnamed x21 -> x1, local copies, waits for them, and re-layouts: 10.7 us -> 1.67 us
    pallas_call x1, Pallas kernels: 60.8 us -> 59.2 us  [per_device(): pl.pallas_call(kernel, out_shape=jax.ShapeDtypeStruct((SEQ_LEN, VALUE_DIM...]
where the time goes in v2:
time: 61.6 us; the launch traced here: 61.5 us
  Pallas kernels  59.2 us (96%)
  local copies, waits for them, and re-layouts  1.67 us (3%)
  between operations  0.66 us (1%)
    pallas_call x1, Pallas kernels, per_device(): pl.pallas_call(kernel, out_shape=jax.ShapeDtypeStruct((SEQ_LEN, VALUE_DIM...  59.2 us
    unnamed x1, local copies, waits for them, and re-layouts  1.67 us

profile of v2, /device:TPU:1, one launch (start us, length us, event | category | flops | bytes accessed | tf_op | source)
XLA Modules:
  0.0 61.5 jit_solution(14938778982010577368)
XLA Ops:
  0.7 59.2 %fused_layer.1 = bf16[512,256]{1,0:T(8,128)(2,1)} custom-call(bf16[512,256]{1,0:T(8,128)(2,1)} %tok.1, bf16[4096,128]{1,0:T(8,128)(2,1)} %wq.1, bf16[4096,128]{1,0:T(8,128)(2,1)} %wk.1, bf16[4096,256]{1,0:T(8,128)(2,1)} %wv.1, bf16[4096,128]{1,0:T(8,128)(2,1)} %wmq.1, bf16[4096,128]{1,0:T(8,128)(2,1)} %wmk.1, bf16[4096,128]{1,0:T(8,128)(2,1)} %wmv.1, ...), custom_call_target="tpu_custom_call" | custom-call | tf_op jit(solution)/shard_map/fused_layer/pallas_call | solution.py:474
  59.8 1.7 %copy.17 = bf16[512,256]{1,0:T(8,128)(2,1)} copy(bf16[512,256]{1,0:T(8,128)(2,1)} %fused_layer.1) | data formatting | bytes 524288

commit v3 on v1

--- a/solution.py
+++ b/solution.py
@@ -49,6 +49,7 @@
 
 
 def kernel(
+    decay,
     tok,
     wq,
     wk,
@@ -61,8 +62,7 @@
     store,
     cos_in,
     sin_in,
-    decay,
-    ids,
+    ids_in,
     out,
     x,
     wt,
@@ -84,11 +84,10 @@
     wl_v,
     cos_v,
     sin_v,
-    out_v,
+    ids,
     ids_all,
     tok_sem,
     local_sem,
-    out_sem,
     z_send,
     z_recv,
     d_send,
@@ -119,6 +118,7 @@
     for copy in tok_copies:
         copy.start()
     local = [
+        (ids_in, ids),
         (wg, wg_v),
         (wq, wt.at[:, pl.ds(0, 128)]),
         (wk, wt.at[:, pl.ds(128, 128)]),
@@ -134,8 +134,7 @@
     local_copies = [
         pltpu.make_async_copy(src, dst, local_sem.at[i]) for i, (src, dst) in enumerate(local)
     ]
-    for copy in local_copies:
-        copy.start()
+    local_copies[0].start()
 
     barrier = pltpu.get_barrier_semaphore()
     for target in (up, down, partner):
@@ -201,6 +200,8 @@
     for copy in tok_copies:
         copy.wait()
     send_own(0)
+    for copy in local_copies[1:]:
+        copy.start()
 
     def id_copy(offset):
         return pltpu.make_async_remote_copy(
@@ -212,14 +213,16 @@
             device_id_type=MESH,
         )
 
+    local_copies[0].wait()
+
     @pl.loop(1, N_ST)
     def _(offset):
         id_copy(offset).start()
 
-    local_copies[0].wait()
+    local_copies[1].wait()
     for chunk in range(RING):
         wg_f[chunk] = wg_v[:, chunk * 512 : (chunk + 1) * 512].astype(F32)
-    for copy in local_copies[1:]:
+    for copy in local_copies[2:]:
         copy.wait()
 
     def add_tokens(chunk, b, first=False):
@@ -387,11 +390,6 @@
         variance = jnp.mean(centred * centred, axis=1, keepdims=True)
         ret_norm[b] = centred * lax.rsqrt(variance + norm_eps)
 
-    def out_copy(b):
-        return pltpu.make_async_copy(
-            out_v.at[b], out.at[pl.ds(b * BLOCK, BLOCK), :], out_sem.at[b]
-        )
-
     def finish_block(b):
         raw = acc_p[b, :, 0:128]
         mean = jnp.mean(raw * raw, axis=1, keepdims=True)
@@ -404,8 +402,7 @@
         lift = dot(mem_out, wl_v[0])
         gate = gate_v[b]
         gate = jnp.concatenate([gate, gate], axis=1)
-        out_v[b] = (ret_norm[b] + gate * lift).astype(BF16)
-        out_copy(b).start()
+        out[b * BLOCK : (b + 1) * BLOCK, :] = (ret_norm[b] + gate * lift).astype(BF16)
 
     for s in range(SLOTS):
         take_slot(1, jnp.int32(s), s < SLOTS - BLOCKS)
@@ -448,9 +445,6 @@
     @pl.loop(0, BLOCKS + 2 * SLOTS)
     def _(n):
         d_copy(1, n, z, 0, core).wait_send()
-
-    for b in range(BLOCKS):
-        out_copy(b).wait()
 
 
 def per_device(
@@ -468,14 +462,28 @@
     passage_ids,
 ):
     cos_table, sin_table = rotary_tables()
-    hbm = pl.BlockSpec(memory_space=pl.ANY)
-    smem = pl.BlockSpec(memory_space=pltpu.SMEM)
+    hbm = pl.BlockSpec(memory_space=pltpu.HBM)
     dma = pltpu.SemaphoreType.DMA
+    operands = (
+        tokens,
+        w_query,
+        w_key,
+        w_value,
+        w_mem_query,
+        w_mem_key,
+        w_mem_value,
+        w_gate.reshape(1, D),
+        w_lift,
+        store,
+        jnp.asarray(cos_table),
+        jnp.asarray(sin_table),
+        passage_ids.T,
+    )
     return pl.pallas_call(
         kernel,
-        out_shape=jax.ShapeDtypeStruct((SEQ_LEN, VALUE_DIM), BF16),
-        in_specs=[hbm] * 12 + [smem] * 2,
-        out_specs=hbm,
+        out_shape=pltpu.VMEM((SEQ_LEN, VALUE_DIM), BF16),
+        in_specs=[pl.BlockSpec(memory_space=pltpu.SMEM)] + [hbm] * 13,
+        out_specs=pl.BlockSpec(memory_space=pltpu.VMEM),
         scratch_shapes=[
             pltpu.VMEM((2, RING, BLOCKS, 2, BLOCK, HALF), BF16),
             pltpu.VMEM((D, TOK_COLS), BF16),
@@ -497,11 +505,10 @@
             pltpu.VMEM((1, MEM_DIM, VALUE_DIM), BF16),
             pltpu.VMEM((SEQ_LEN, KEY_DIM), F32),
             pltpu.VMEM((SEQ_LEN, KEY_DIM), F32),
-            pltpu.VMEM((BLOCKS, BLOCK, VALUE_DIM), BF16),
+            pltpu.SMEM((PICKS, BLOCKS), jnp.int32),
             pltpu.SMEM((N_ST, PICKS, BLOCKS), jnp.int32),
             dma((BLOCKS,)),
-            dma((11,)),
-            dma((BLOCKS,)),
+            dma((12,)),
             dma((2, 2, SLOTS)),
             dma((2, 2, SLOTS)),
             dma((2, BLOCKS + 2 * SLOTS)),
@@ -515,22 +522,7 @@
             collective_id=0, has_side_effects=True, vmem_limit_bytes=48 * 1024 * 1024
         ),
         name="fused_layer",
-    )(
-        tokens,
-        w_query,
-        w_key,
-        w_value,
-        w_mem_query,
-        w_mem_key,
-        w_mem_value,
-        w_gate.reshape(1, D),
-        w_lift,
-        store,
-        cos_table,
-        sin_table,
-        decay_rate,
-        passage_ids.T,
-    )
+    )(decay_rate, *[pltpu.with_memory_space_constraint(array, pltpu.HBM) for array in operands])
 
 
 def solution(mesh):

time: 72.6 us -> 59.5 us (0.82)
  local copies, waits for them, and re-layouts: 10.7 us -> 0.71 us
  Pallas kernels: 60.8 us -> 58 us
    unnamed x21 -> x1, local copies, waits for them, and re-layouts: 10.7 us -> 0.71 us
    pallas_call x1, Pallas kernels: 60.8 us -> 58 us  [per_device(): pl.pallas_call(kernel, out_shape=pltpu.VMEM((SEQ_LEN, VALUE_DIM), BF16),...]
where the time goes in v3:
time: 59.5 us; the launch traced here: 59.3 us
  Pallas kernels  58 us (97%)
  local copies, waits for them, and re-layouts  0.71 us (1%)
  between operations  0.66 us (1%)
    pallas_call x1, Pallas kernels, per_device(): pl.pallas_call(kernel, out_shape=pltpu.VMEM((SEQ_LEN, VALUE_DIM), BF16),...  58 us

profile of v3, /device:TPU:1, one launch (start us, length us, event | category | flops | bytes accessed | tf_op | source)
XLA Modules:
  0.0 59.3 jit_solution(3316995871767386291)
XLA Ops:
  0.7 58.0 %fused_layer.1 = bf16[512,256]{1,0:T(8,128)(2,1)S(1)} custom-call(f32[1]{0:T(128)S(6)} %copy.17.decay, bf16[512,256]{1,0:T(8,128)(2,1)} %tok.1, bf16[4096,128]{1,0:T(8,128)(2,1)} %wq.1, bf16[4096,128]{1,0:T(8,128)(2,1)} %wk.1, bf16[4096,256]{1,0:T(8,128)(2,1)} %wv.1, bf16[4096,128]{1,0:T(8,128)(2,1)} %wmq.1, bf16[4096,128]{1,0:T(8,128)(2,1)} %wmk.1, ...), custom_call_target="tpu_custom_call" | custom-call | tf_op jit(solution)/shard_map/fused_layer/pallas_call | solution.py:482
  58.6 0.7 %copy.16 = bf16[512,256]{1,0:T(8,128)(2,1)} copy(bf16[512,256]{1,0:T(8,128)(2,1)S(1)} %fused_layer.1) | data formatting | bytes 524288

commit v4 on v3

--- a/solution.py
+++ b/solution.py
@@ -21,6 +21,12 @@
 SLOTS = 14
 HALF = 256
 TOK_COLS = 640
+
+STEPS = sorted(
+    ((a, b) for a in range(4) for b in range(4) if a or b),
+    key=lambda step: sum(min(part, 4 - part) for part in step),
+)
+RINGS = [range(0, 4), range(4, 10), range(10, 14), range(14, 15)]
 
 norm_eps = 1e-06
 rope_base = 10000.0
@@ -96,6 +102,7 @@
     i_recv,
     s_send,
     s_recv,
+    meet_sem,
 ):
     st = lax.axis_index("st")
     tp = lax.axis_index("tp")
@@ -106,8 +113,20 @@
     down = lax.rem(z + RING - 1, RING) * 2 + core
     partner = z * 2 + other
 
-    def peer(offset):
-        return lax.rem(st + offset, N_ST)
+    side = 4
+    row, column = lax.div(st, side), lax.rem(st, side)
+
+    def peer(place):
+        down_by, right_by = STEPS[place]
+        return lax.rem(row + down_by, side) * side + lax.rem(column + right_by, side)
+
+    def source(place):
+        down_by, right_by = STEPS[place]
+        return lax.rem(row + side - down_by, side) * side + lax.rem(
+            column + side - right_by, side
+        )
+
+    near = [peer(place) for place in RINGS[0]]
 
     tok_copies = [
         pltpu.make_async_copy(
@@ -119,12 +138,12 @@
         copy.start()
     local = [
         (ids_in, ids),
+        (store, store_v),
         (wg, wg_v),
         (wq, wt.at[:, pl.ds(0, 128)]),
         (wk, wt.at[:, pl.ds(128, 128)]),
         (wv, wt.at[:, pl.ds(256, 256)]),
         (wmq, wt.at[:, pl.ds(512, 128)]),
-        (store, store_v),
         (wmk, wm.at[:, pl.ds(0, 128)]),
         (wmv, wm.at[:, pl.ds(128, 128)]),
         (wl, wl_v),
@@ -139,14 +158,20 @@
     barrier = pltpu.get_barrier_semaphore()
     for target in (up, down, partner):
         pl.semaphore_signal(barrier, inc=1, device_id={"tp": target}, device_id_type=MESH)
-
-    @pl.loop(1, N_ST)
-    def _(offset):
-        pl.semaphore_signal(
-            barrier, inc=1, device_id={"st": peer(offset)}, device_id_type=MESH
-        )
-
-    pl.semaphore_wait(barrier, 3 + N_ST - 1)
+    for target in near:
+        pl.semaphore_signal(barrier, inc=1, device_id={"st": target}, device_id_type=MESH)
+    pl.semaphore_wait(barrier, 3 + len(near))
+
+    def tell(step):
+        for target in near:
+            pl.semaphore_signal(
+                meet_sem.at[step], inc=1, device_id={"st": target}, device_id_type=MESH
+            )
+
+    def meet(step):
+        pl.semaphore_wait(meet_sem.at[step], len(near))
+
+    tell(0)
 
     def slot_block(d, s):
         return lax.rem(s + 2 * d, BLOCKS)
@@ -203,27 +228,49 @@
     for copy in local_copies[1:]:
         copy.start()
 
-    def id_copy(offset):
+    def id_copy(place, slot):
         return pltpu.make_async_remote_copy(
             src_ref=ids,
-            dst_ref=ids_all.at[st],
-            send_sem=i_send.at[offset],
-            recv_sem=i_recv.at[offset],
-            device_id={"st": peer(offset)},
+            dst_ref=ids_all.at[slot],
+            send_sem=i_send.at[place],
+            recv_sem=i_recv.at[place],
+            device_id={"st": peer(place)},
             device_id_type=MESH,
         )
 
-    local_copies[0].wait()
-
-    @pl.loop(1, N_ST)
-    def _(offset):
-        id_copy(offset).start()
-
-    local_copies[1].wait()
-    for chunk in range(RING):
-        wg_f[chunk] = wg_v[:, chunk * 512 : (chunk + 1) * 512].astype(F32)
-    for copy in local_copies[2:]:
-        copy.wait()
+    def row_copy(place, slot):
+        return pltpu.make_async_remote_copy(
+            src_ref=outbox.at[place],
+            dst_ref=inbox.at[slot],
+            send_sem=s_send.at[place],
+            recv_sem=s_recv.at[place],
+            device_id={"st": peer(place)},
+            device_id_type=MESH,
+        )
+
+    def wanted_row(read):
+        wanted = jnp.int32(0)
+        for pick in range(PICKS):
+            for b in range(BLOCKS):
+                ident = read(pick, b)
+                mine = lax.shift_right_logical(ident, PASS_SHIFT) == st
+                wanted = wanted + jnp.where(mine, ident & ((1 << PASS_SHIFT) - 1), 0)
+        return wanted
+
+    def send_ids(ring):
+        for place in RINGS[ring]:
+            id_copy(place, st).start()
+
+    def gather_rows(ring):
+        for place in RINGS[ring]:
+            id_copy(place, source(place)).wait_recv()
+        for place in RINGS[ring]:
+            target = peer(place)
+            outbox[place] = store_v[wanted_row(lambda pick, b: ids_all[target, pick, b])]
+
+    def send_rows(ring):
+        for place in RINGS[ring]:
+            row_copy(place, st).start()
 
     def add_tokens(chunk, b, first=False):
         both = jnp.concatenate([x[0, chunk, b, 0], x[0, chunk, b, 1]], axis=1)
@@ -278,81 +325,78 @@
             else:
                 add_passages(chunk, b)
 
-    for b in range(BLOCKS):
+    def add_own_tokens(b):
         d_copy(0, b, z, b, other).wait_recv()
         add_tokens(z, b, first=True)
 
-    def id_arrival(offset):
-        return pltpu.make_async_remote_copy(
-            src_ref=ids,
-            dst_ref=ids_all.at[peer(N_ST - offset)],
-            send_sem=i_send.at[offset],
-            recv_sem=i_recv.at[offset],
-            device_id={"st": peer(offset)},
-            device_id_type=MESH,
-        )
-
-    take_slot(0, jnp.int32(0), True)
-
-    @pl.loop(1, N_ST)
-    def _(offset):
-        id_arrival(offset).wait_recv()
-
-    def wanted_row(read):
-        row = jnp.int32(0)
-        for pick in range(PICKS):
-            for b in range(BLOCKS):
-                ident = read(pick, b)
-                mine = lax.shift_right_logical(ident, PASS_SHIFT) == st
-                row = row + jnp.where(mine, ident & ((1 << PASS_SHIFT) - 1), 0)
-        return row
-
+    def take(s):
+        take_slot(0, jnp.int32(s), True)
+
+    def add(s):
+        add_slot(0, jnp.int32(s))
+
+    local_copies[0].wait()
+    send_ids(0)
+    meet(0)
+    tell(1)
+    send_ids(1)
+    take(0)
+    meet(1)
+    tell(2)
+    send_ids(2)
+    take(1)
+    meet(2)
+    send_ids(3)
+    local_copies[1].wait()
     inbox[st] = store_v[wanted_row(lambda pick, b: ids[pick, b])]
-
-    @pl.loop(1, N_ST)
-    def _(offset):
-        target = peer(offset)
-        outbox[offset] = store_v[wanted_row(lambda pick, b: ids_all[target, pick, b])]
-
-    take_slot(0, jnp.int32(1), True)
-    add_slot(0, jnp.int32(0))
-
-    def row_copy(offset, place):
-        return pltpu.make_async_remote_copy(
-            src_ref=outbox.at[offset],
-            dst_ref=inbox.at[place],
-            send_sem=s_send.at[offset],
-            recv_sem=s_recv.at[offset],
-            device_id={"st": peer(offset)},
-            device_id_type=MESH,
-        )
-
-    @pl.loop(1, N_ST)
-    def _(offset):
-        row_copy(offset, st).start()
-
-    @pl.loop(2, 9)
+    take(2)
+    gather_rows(0)
+    take(3)
+    send_rows(0)
+    gather_rows(1)
+    take(4)
+    send_rows(1)
+    gather_rows(2)
+    take(5)
+    send_rows(2)
+    gather_rows(3)
+    for copy in local_copies[2:]:
+        copy.wait()
+    for chunk in range(RING):
+        wg_f[chunk] = wg_v[:, chunk * 512 : (chunk + 1) * 512].astype(F32)
+    add_own_tokens(0)
+    add_own_tokens(1)
+    take(6)
+    send_rows(3)
+    add_own_tokens(2)
+    add_own_tokens(3)
+    add(0)
+
+    @pl.loop(7, 10)
     def _(s):
         take_slot(0, s, True)
-        add_slot(0, s - 1)
-
-    @pl.loop(1, N_ST)
-    def _(offset):
-        row_copy(offset, peer(N_ST - offset)).wait_recv()
-
+
+        @pl.loop(0, jnp.where(s < 9, 3, 2))
+        def _(n):
+            add_slot(0, 1 + 3 * (s - 7) + n)
+
+    for place in range(N_ST - 1):
+        row_copy(place, source(place)).wait_recv()
     for b in range(BLOCKS):
         for pick in range(PICKS):
             owner = lax.shift_right_logical(ids[pick, b], PASS_SHIFT)
             x[1, z, b, core, pick * PASS_ROWS : (pick + 1) * PASS_ROWS, :] = inbox[owner]
 
-    take_slot(0, jnp.int32(9), True)
-    add_slot(0, jnp.int32(8))
+    add_slot(0, jnp.int32(9))
     send_own(1)
 
     @pl.loop(10, SLOTS)
     def _(s):
         take_slot(0, s, False)
-        add_slot(0, s - 1)
+
+        @pl.when(s > 10)
+        def _():
+            add_slot(0, s - 1)
 
     rate = decay[0]
 
@@ -426,10 +470,9 @@
             def _(n):
                 d_copy(0, n, z, 0, core).wait_send()
 
-            @pl.loop(1, N_ST)
-            def _(offset):
-                id_copy(offset).wait_send()
-                row_copy(offset, st).wait_send()
+            for place in range(N_ST - 1):
+                id_copy(place, st).wait_send()
+                row_copy(place, st).wait_send()
 
     finish_block(0)
     finish_block(2)
@@ -517,6 +560,7 @@
             dma((N_ST,)),
             dma((N_ST,)),
             dma((N_ST,)),
+            pltpu.SemaphoreType.REGULAR((3,)),
         ],
         compiler_params=pltpu.CompilerParams(
             collective_id=0, has_side_effects=True, vmem_limit_bytes=48 * 1024 * 1024

time: 59.5 us -> 57 us (0.958)
  Pallas kernels: 58 us -> 55.5 us
    pallas_call x1, Pallas kernels: 58 us -> 55.5 us  [per_device(): pl.pallas_call(kernel, out_shape=pltpu.VMEM((SEQ_LEN, VALUE_DIM), BF16),...]
where the time goes in v4:
time: 57 us; the launch traced here: 56.9 us
  Pallas kernels  55.5 us (97%)
  local copies, waits for them, and re-layouts  0.71 us (1%)
  between operations  0.66 us (1%)
    pallas_call x1, Pallas kernels, per_device(): pl.pallas_call(kernel, out_shape=pltpu.VMEM((SEQ_LEN, VALUE_DIM), BF16),...  55.5 us

profile of v4, /device:TPU:1, one launch (start us, length us, event | category | flops | bytes accessed | tf_op | source)
XLA Modules:
  0.0 56.9 jit_solution(18277003881035064288)
XLA Ops:
  0.7 55.5 %fused_layer.1 = bf16[512,256]{1,0:T(8,128)(2,1)S(1)} custom-call(f32[1]{0:T(128)S(6)} %copy.17.decay, bf16[512,256]{1,0:T(8,128)(2,1)} %tok.1, bf16[4096,128]{1,0:T(8,128)(2,1)} %wq.1, bf16[4096,128]{1,0:T(8,128)(2,1)} %wk.1, bf16[4096,256]{1,0:T(8,128)(2,1)} %wv.1, bf16[4096,128]{1,0:T(8,128)(2,1)} %wmq.1, bf16[4096,128]{1,0:T(8,128)(2,1)} %wmk.1, ...), custom_call_target="tpu_custom_call" | custom-call | tf_op jit(solution)/shard_map/fused_layer/pallas_call | solution.py:525
  56.2 0.7 %copy.16 = bf16[512,256]{1,0:T(8,128)(2,1)} copy(bf16[512,256]{1,0:T(8,128)(2,1)S(1)} %fused_layer.1) | data formatting | bytes 524288

commit v5 on v4

--- a/solution.py
+++ b/solution.py
@@ -19,6 +19,7 @@
 RING = 8
 BLOCKS = 4
 SLOTS = 14
+PAIRS = SLOTS // 2
 HALF = 256
 TOK_COLS = 640
 
@@ -126,11 +127,16 @@
             column + side - right_by, side
         )
 
-    near = [peer(place) for place in RINGS[0]]
+    near = (
+        lax.rem(row + 1, side) * side + column,
+        lax.rem(row + side - 1, side) * side + column,
+        row * side + lax.rem(column + 1, side),
+        row * side + lax.rem(column + side - 1, side),
+    )
 
     tok_copies = [
         pltpu.make_async_copy(
-            tok.at[pl.ds(b * BLOCK, BLOCK), :], x.at[0, z, b, core], tok_sem.at[b]
+            tok.at[pl.ds(b * BLOCK, BLOCK), :], x.at[0, z, core, b], tok_sem.at[b]
         )
         for b in range(BLOCKS)
     ]
@@ -158,18 +164,39 @@
     barrier = pltpu.get_barrier_semaphore()
     for target in (up, down, partner):
         pl.semaphore_signal(barrier, inc=1, device_id={"tp": target}, device_id_type=MESH)
-    for target in near:
-        pl.semaphore_signal(barrier, inc=1, device_id={"st": target}, device_id_type=MESH)
-    pl.semaphore_wait(barrier, 3 + len(near))
+    ahead = (row < side - 1, row == 0, column < side - 1, column == 0)
+    behind = (row == side - 1, row > 0, column == side - 1, column > 0)
+    for target, chosen in zip(near, ahead):
+
+        @pl.when(chosen)
+        def _():
+            pl.semaphore_signal(barrier, inc=1, device_id={"st": target}, device_id_type=MESH)
+
+    early = sum(one.astype(jnp.int32) for one in behind)
+    pl.semaphore_wait(barrier, 3 + early)
 
     def tell(step):
-        for target in near:
-            pl.semaphore_signal(
-                meet_sem.at[step], inc=1, device_id={"st": target}, device_id_type=MESH
-            )
+        for target, chosen in zip(near, behind):
+
+            def signal():
+                pl.semaphore_signal(
+                    meet_sem.at[step], inc=1, device_id={"st": target}, device_id_type=MESH
+                )
+
+            if step == 0:
+                pl.when(chosen)(signal)
+            else:
+                signal()
 
     def meet(step):
-        pl.semaphore_wait(meet_sem.at[step], len(near))
+        if step == 0:
+
+            @pl.when(early < len(near))
+            def _():
+                pl.semaphore_wait(meet_sem.at[0], len(near) - early)
+
+        else:
+            pl.semaphore_wait(meet_sem.at[step], len(near))
 
     tell(0)
 
@@ -180,7 +207,7 @@
         return lax.rem(z + RING - hops, RING) if d == 0 else lax.rem(z + hops, RING)
 
     def z_copy(phase, d, s):
-        ref = x.at[phase, chunk_at(d, lax.div(s, BLOCKS)), slot_block(d, s), core]
+        ref = x.at[phase, chunk_at(d, lax.div(s, BLOCKS)), core, slot_block(d, s)]
         return pltpu.make_async_remote_copy(
             src_ref=ref,
             dst_ref=ref,
@@ -191,7 +218,7 @@
         )
 
     def z_arrival(phase, d, s):
-        ref = x.at[phase, chunk_at(d, lax.div(s, BLOCKS) + 1), slot_block(d, s), core]
+        ref = x.at[phase, chunk_at(d, lax.div(s, BLOCKS) + 1), core, slot_block(d, s)]
         return pltpu.make_async_remote_copy(
             src_ref=ref,
             dst_ref=ref,
@@ -201,8 +228,8 @@
             device_id_type=MESH,
         )
 
-    def d_copy(phase, index, chunk, b, half):
-        ref = x.at[phase, chunk, b, half]
+    def d_copy(phase, index, chunk, b, half, count=2):
+        ref = x.at[phase, chunk, half, pl.ds(b, count)]
         return pltpu.make_async_remote_copy(
             src_ref=ref,
             dst_ref=ref,
@@ -212,15 +239,25 @@
             device_id_type=MESH,
         )
 
-    def d_slot(d, s):
-        return BLOCKS + d * SLOTS + s
+    def own_copy(phase, pair, half):
+        return d_copy(phase, pair, z, 2 * pair, half)
+
+    def pair_copy(phase, d, pair, half):
+        s = 2 * pair
+        chunk = chunk_at(d, lax.div(s, BLOCKS) + 1)
+        return d_copy(phase, 2 + d * PAIRS + pair, chunk, slot_block(d, s), half)
+
+    def slot_copy(phase, d, s, half):
+        chunk = chunk_at(d, lax.div(s, BLOCKS) + 1)
+        index = 2 + 2 * PAIRS + 2 * d + s - (SLOTS - 2)
+        return d_copy(phase, index, chunk, slot_block(d, s), half, 1)
 
     def send_own(phase):
         for b in range(BLOCKS):
             z_copy(phase, 0, jnp.int32(b)).start()
             z_copy(phase, 1, jnp.int32(b)).start()
-        for b in range(BLOCKS):
-            d_copy(phase, b, z, b, core).start()
+        for pair in range(2):
+            own_copy(phase, pair, core).start()
 
     for copy in tok_copies:
         copy.wait()
@@ -273,7 +310,7 @@
             row_copy(place, st).start()
 
     def add_tokens(chunk, b, first=False):
-        both = jnp.concatenate([x[0, chunk, b, 0], x[0, chunk, b, 1]], axis=1)
+        both = jnp.concatenate([x[0, chunk, 0, b], x[0, chunk, 1, b]], axis=1)
         rows = pl.ds(pl.multiple_of(chunk * 512, 512), 512)
         product = dot(both, wt[rows, :])
         wide = both.astype(F32)
@@ -293,7 +330,7 @@
             gates[b] += gated
 
     def add_passages(chunk, b, first=False):
-        both = jnp.concatenate([x[1, chunk, b, 0], x[1, chunk, b, 1]], axis=1)
+        both = jnp.concatenate([x[1, chunk, 0, b], x[1, chunk, 1, b]], axis=1)
         rows = pl.ds(pl.multiple_of(chunk * 512, 512), 512)
         product = dot(both, wm[rows, :])
         if first:
@@ -304,99 +341,129 @@
     def take_slot(phase, s, relay):
         for d in range(2):
             z_arrival(phase, d, s).wait_recv()
-            if relay is True:
+            if relay:
                 z_copy(phase, d, s + BLOCKS).start()
-            elif relay is not False:
-
-                @pl.when(relay)
-                def _():
-                    z_copy(phase, d, s + BLOCKS).start()
-
-            chunk = chunk_at(d, lax.div(s, BLOCKS) + 1)
-            d_copy(phase, d_slot(d, s), chunk, slot_block(d, s), core).start()
+
+    def add_one(phase, d, s):
+        chunk = chunk_at(d, lax.div(s, BLOCKS) + 1)
+        if phase == 0:
+            add_tokens(chunk, slot_block(d, s))
+        else:
+            add_passages(chunk, slot_block(d, s))
+
+    def hand_pair(phase, pair):
+        for d in range(2):
+            pair_copy(phase, d, pair, core).start()
+
+    def add_pair(phase, pair):
+        for d in range(2):
+            pair_copy(phase, d, pair, other).wait_recv()
+            add_one(phase, d, 2 * pair)
+            add_one(phase, d, 2 * pair + 1)
+
+    def hand_slot(phase, s):
+        for d in range(2):
+            slot_copy(phase, d, s, core).start()
 
     def add_slot(phase, s):
         for d in range(2):
-            chunk = chunk_at(d, lax.div(s, BLOCKS) + 1)
-            b = slot_block(d, s)
-            d_copy(phase, d_slot(d, s), chunk, b, other).wait_recv()
-            if phase == 0:
-                add_tokens(chunk, b)
-            else:
-                add_passages(chunk, b)
-
-    def add_own_tokens(b):
-        d_copy(0, b, z, b, other).wait_recv()
-        add_tokens(z, b, first=True)
+            slot_copy(phase, d, s, other).wait_recv()
+            add_one(phase, d, s)
+
+    def add_own_tokens(pair):
+        own_copy(0, pair, other).wait_recv()
+        add_tokens(z, 2 * pair, first=True)
+        add_tokens(z, 2 * pair + 1, first=True)
 
     def take(s):
-        take_slot(0, jnp.int32(s), True)
-
-    def add(s):
-        add_slot(0, jnp.int32(s))
+        take_slot(0, jnp.int32(s), s < SLOTS - BLOCKS)
+        if s % 2:
+            hand_pair(0, jnp.int32(s // 2))
+
+    def add(pair):
+        add_pair(0, jnp.int32(pair))
+
+    late = jnp.minimum(row, 2) + jnp.minimum(column, 2) >= 2
+    soon = jnp.logical_not(late)
+
+    def greet(ring):
+        meet(ring)
+        if ring + 1 < len(RINGS):
+            tell(ring + 1)
+        send_ids(ring)
+
+    def gather_all():
+        for ring in range(len(RINGS)):
+            gather_rows(ring)
+
+    def send_all():
+        for ring in range(len(RINGS)):
+            send_rows(ring)
 
     local_copies[0].wait()
-    send_ids(0)
-    meet(0)
-    tell(1)
-    send_ids(1)
+    greet(0)
+
+    @pl.when(late)
+    def _():
+        greet(1)
+        greet(2)
+        greet(3)
+
     take(0)
-    meet(1)
-    tell(2)
-    send_ids(2)
+
+    @pl.when(soon)
+    def _():
+        greet(1)
+
     take(1)
-    meet(2)
-    send_ids(3)
+
+    @pl.when(soon)
+    def _():
+        greet(2)
+
     local_copies[1].wait()
     inbox[st] = store_v[wanted_row(lambda pick, b: ids[pick, b])]
     take(2)
-    gather_rows(0)
+
+    @pl.when(soon)
+    def _():
+        greet(3)
+
     take(3)
-    send_rows(0)
-    gather_rows(1)
+    pl.when(late)(gather_all)
     take(4)
-    send_rows(1)
-    gather_rows(2)
+    pl.when(late)(send_all)
     take(5)
-    send_rows(2)
-    gather_rows(3)
+    pl.when(soon)(gather_all)
     for copy in local_copies[2:]:
         copy.wait()
     for chunk in range(RING):
         wg_f[chunk] = wg_v[:, chunk * 512 : (chunk + 1) * 512].astype(F32)
     add_own_tokens(0)
+    take(6)
+    pl.when(soon)(send_all)
     add_own_tokens(1)
-    take(6)
-    send_rows(3)
-    add_own_tokens(2)
-    add_own_tokens(3)
     add(0)
-
-    @pl.loop(7, 10)
-    def _(s):
-        take_slot(0, s, True)
-
-        @pl.loop(0, jnp.where(s < 9, 3, 2))
-        def _(n):
-            add_slot(0, 1 + 3 * (s - 7) + n)
-
+    take(7)
+    add(1)
+    take(8)
+    add(2)
+    take(9)
     for place in range(N_ST - 1):
         row_copy(place, source(place)).wait_recv()
     for b in range(BLOCKS):
         for pick in range(PICKS):
             owner = lax.shift_right_logical(ids[pick, b], PASS_SHIFT)
-            x[1, z, b, core, pick * PASS_ROWS : (pick + 1) * PASS_ROWS, :] = inbox[owner]
-
-    add_slot(0, jnp.int32(9))
+            x[1, z, core, b, pick * PASS_ROWS : (pick + 1) * PASS_ROWS, :] = inbox[owner]
+
+    add(3)
     send_own(1)
-
-    @pl.loop(10, SLOTS)
-    def _(s):
-        take_slot(0, s, False)
-
-        @pl.when(s > 10)
-        def _():
-            add_slot(0, s - 1)
+    take(10)
+    add(4)
+    take(11)
+    take(12)
+    add(5)
+    take(13)
 
     rate = decay[0]
 
@@ -448,25 +515,31 @@
         gate = jnp.concatenate([gate, gate], axis=1)
         out[b * BLOCK : (b + 1) * BLOCK, :] = (ret_norm[b] + gate * lift).astype(BF16)
 
-    for s in range(SLOTS):
-        take_slot(1, jnp.int32(s), s < SLOTS - BLOCKS)
-        if s == 0:
-            add_slot(0, jnp.int32(SLOTS - 1))
-            for b in range(BLOCKS):
-                d_copy(1, b, z, b, other).wait_recv()
-                add_passages(z, b, first=True)
-        else:
-            add_slot(1, jnp.int32(s - 1))
-        if s < BLOCKS:
-            finish_tokens(s)
-        if s == 8:
+    for step in range(SLOTS):
+        s = jnp.int32(step)
+        take_slot(1, s, step < SLOTS - BLOCKS)
+        if step >= SLOTS - 2:
+            hand_slot(1, s)
+        elif step % 2:
+            hand_pair(1, jnp.int32(step // 2))
+        if step == 0:
+            add(PAIRS - 1)
+            for pair in range(2):
+                own_copy(1, pair, other).wait_recv()
+                add_passages(z, 2 * pair, first=True)
+                add_passages(z, 2 * pair + 1, first=True)
+        elif step % 2 == 0:
+            add_pair(1, jnp.int32(step // 2 - 1))
+        if step < BLOCKS:
+            finish_tokens(step)
+        if step == 8:
 
             @pl.loop(0, SLOTS)
             def _(n):
                 z_copy(0, 0, n).wait_send()
                 z_copy(0, 1, n).wait_send()
 
-            @pl.loop(0, BLOCKS + 2 * SLOTS)
+            @pl.loop(0, 2 + 2 * PAIRS)
             def _(n):
                 d_copy(0, n, z, 0, core).wait_send()
 
@@ -474,6 +547,7 @@
                 id_copy(place, st).wait_send()
                 row_copy(place, st).wait_send()
 
+    add_slot(1, jnp.int32(SLOTS - 2))
     finish_block(0)
     finish_block(2)
     add_slot(1, jnp.int32(SLOTS - 1))
@@ -485,9 +559,14 @@
         z_copy(1, 0, n).wait_send()
         z_copy(1, 1, n).wait_send()
 
-    @pl.loop(0, BLOCKS + 2 * SLOTS)
-    def _(n):
-        d_copy(1, n, z, 0, core).wait_send()
+    for pair in range(2):
+        own_copy(1, pair, core).wait_send()
+    for pair in range(PAIRS - 1):
+        for d in range(2):
+            pair_copy(1, d, pair, core).wait_send()
+    for s in (SLOTS - 2, SLOTS - 1):
+        for d in range(2):
+            slot_copy(1, d, s, core).wait_send()
 
 
 def per_device(
@@ -528,7 +607,7 @@
         in_specs=[pl.BlockSpec(memory_space=pltpu.SMEM)] + [hbm] * 13,
         out_specs=pl.BlockSpec(memory_space=pltpu.VMEM),
         scratch_shapes=[
-            pltpu.VMEM((2, RING, BLOCKS, 2, BLOCK, HALF), BF16),
+            pltpu.VMEM((2, RING, 2, BLOCKS, BLOCK, HALF), BF16),
             pltpu.VMEM((D, TOK_COLS), BF16),
             pltpu.VMEM((D, 2 * MEM_DIM), BF16),
             pltpu.VMEM(store.shape, BF16),
@@ -554,13 +633,13 @@
             dma((12,)),
             dma((2, 2, SLOTS)),
             dma((2, 2, SLOTS)),
-            dma((2, BLOCKS + 2 * SLOTS)),
-            dma((2, BLOCKS + 2 * SLOTS)),
+            dma((2, 6 + 2 * PAIRS)),
+            dma((2, 6 + 2 * PAIRS)),
             dma((N_ST,)),
             dma((N_ST,)),
             dma((N_ST,)),
             dma((N_ST,)),
-            pltpu.SemaphoreType.REGULAR((3,)),
+            pltpu.SemaphoreType.REGULAR((4,)),
         ],
         compiler_params=pltpu.CompilerParams(
             collective_id=0, has_side_effects=True, vmem_limit_bytes=48 * 1024 * 1024

time: 57 us -> 55.5 us (0.974)
  Pallas kernels: 55.5 us -> 54 us
    pallas_call x1, Pallas kernels: 55.5 us -> 54 us  [per_device(): pl.pallas_call(kernel, out_shape=pltpu.VMEM((SEQ_LEN, VALUE_DIM), BF16),...]
where the time goes in v5:
time: 55.5 us; the launch traced here: 55.3 us
  Pallas kernels  54 us (97%)
  local copies, waits for them, and re-layouts  0.71 us (1%)
  between operations  0.66 us (1%)
    pallas_call x1, Pallas kernels, per_device(): pl.pallas_call(kernel, out_shape=pltpu.VMEM((SEQ_LEN, VALUE_DIM), BF16),...  54 us

profile of v5, /device:TPU:1, one launch (start us, length us, event | category | flops | bytes accessed | tf_op | source)
XLA Modules:
  0.0 55.3 jit_solution(6961859765110203470)
XLA Ops:
  0.7 54.0 %fused_layer.1 = bf16[512,256]{1,0:T(8,128)(2,1)S(1)} custom-call(f32[1]{0:T(128)S(6)} %copy.17.decay, bf16[512,256]{1,0:T(8,128)(2,1)} %tok.1, bf16[4096,128]{1,0:T(8,128)(2,1)} %wq.1, bf16[4096,128]{1,0:T(8,128)(2,1)} %wk.1, bf16[4096,256]{1,0:T(8,128)(2,1)} %wv.1, bf16[4096,128]{1,0:T(8,128)(2,1)} %wmq.1, bf16[4096,128]{1,0:T(8,128)(2,1)} %wmk.1, ...), custom_call_target="tpu_custom_call" | custom-call | tf_op jit(solution)/shard_map/fused_layer/pallas_call | solution.py:604
  54.6 0.7 %copy.16 = bf16[512,256]{1,0:T(8,128)(2,1)} copy(bf16[512,256]{1,0:T(8,128)(2,1)S(1)} %fused_layer.1) | data formatting | bytes 524288

commit v6 on v5

--- a/solution.py
+++ b/solution.py
@@ -19,7 +19,6 @@
 RING = 8
 BLOCKS = 4
 SLOTS = 14
-PAIRS = SLOTS // 2
 HALF = 256
 TOK_COLS = 640
 
@@ -228,36 +227,24 @@
             device_id_type=MESH,
         )
 
-    def d_copy(phase, index, chunk, b, half, count=2):
-        ref = x.at[phase, chunk, half, pl.ds(b, count)]
+    def hand_copy(phase, d, s, half, count):
+        chunk = chunk_at(d, s // BLOCKS + 1)
+        ref = x.at[phase, chunk, half, pl.ds((s + 2 * d) % BLOCKS, count)] if count < BLOCKS else x.at[phase, chunk, half]
+        index = BLOCKS + s
         return pltpu.make_async_remote_copy(
             src_ref=ref,
             dst_ref=ref,
-            send_sem=d_send.at[phase, index],
-            recv_sem=d_recv.at[phase, index],
+            send_sem=d_send.at[phase, d, index],
+            recv_sem=d_recv.at[phase, d, index],
             device_id={"tp": partner},
             device_id_type=MESH,
         )
-
-    def own_copy(phase, pair, half):
-        return d_copy(phase, pair, z, 2 * pair, half)
-
-    def pair_copy(phase, d, pair, half):
-        s = 2 * pair
-        chunk = chunk_at(d, lax.div(s, BLOCKS) + 1)
-        return d_copy(phase, 2 + d * PAIRS + pair, chunk, slot_block(d, s), half)
-
-    def slot_copy(phase, d, s, half):
-        chunk = chunk_at(d, lax.div(s, BLOCKS) + 1)
-        index = 2 + 2 * PAIRS + 2 * d + s - (SLOTS - 2)
-        return d_copy(phase, index, chunk, slot_block(d, s), half, 1)
 
     def send_own(phase):
         for b in range(BLOCKS):
             z_copy(phase, 0, jnp.int32(b)).start()
             z_copy(phase, 1, jnp.int32(b)).start()
-        for pair in range(2):
-            own_copy(phase, pair, core).start()
+        hand_copy(phase, 0, -BLOCKS, core, BLOCKS).start()
 
     for copy in tok_copies:
         copy.wait()
@@ -351,37 +338,33 @@
         else:
             add_passages(chunk, slot_block(d, s))
 
-    def hand_pair(phase, pair):
-        for d in range(2):
-            pair_copy(phase, d, pair, core).start()
-
-    def add_pair(phase, pair):
-        for d in range(2):
-            pair_copy(phase, d, pair, other).wait_recv()
-            add_one(phase, d, 2 * pair)
-            add_one(phase, d, 2 * pair + 1)
-
-    def hand_slot(phase, s):
-        for d in range(2):
-            slot_copy(phase, d, s, core).start()
-
-    def add_slot(phase, s):
-        for d in range(2):
-            slot_copy(phase, d, s, other).wait_recv()
-            add_one(phase, d, s)
-
-    def add_own_tokens(pair):
-        own_copy(0, pair, other).wait_recv()
-        add_tokens(z, 2 * pair, first=True)
-        add_tokens(z, 2 * pair + 1, first=True)
-
-    def take(s):
-        take_slot(0, jnp.int32(s), s < SLOTS - BLOCKS)
-        if s % 2:
-            hand_pair(0, jnp.int32(s // 2))
-
-    def add(pair):
-        add_pair(0, jnp.int32(pair))
+    hand_groups = (
+        ((0, 2), (2, 2), (4, 2), (6, 2), (8, 2), (10, 2), (12, 2)),
+        ((0, 2), (2, 2), (4, 2), (6, 2), (8, 2), (10, 2), (12, 1), (13, 1)),
+    )
+
+    def take(phase, s):
+        take_slot(phase, jnp.int32(s), s < SLOTS - BLOCKS)
+        for first, count in hand_groups[phase]:
+            if s == first + count - 1:
+                for d in range(2):
+                    hand_copy(phase, d, first, core, count).start()
+
+    def add(phase, *slots):
+        for s in slots:
+            for d in range(2):
+                for first, count in hand_groups[phase]:
+                    if s == first:
+                        hand_copy(phase, d, first, other, count).wait_recv()
+                add_one(phase, d, jnp.int32(s))
+
+    def add_own(phase):
+        hand_copy(phase, 0, -BLOCKS, other, BLOCKS).wait_recv()
+        for b in range(BLOCKS):
+            if phase == 0:
+                add_tokens(z, b, first=True)
+            else:
+                add_passages(z, b, first=True)
 
     late = jnp.minimum(row, 2) + jnp.minimum(column, 2) >= 2
     soon = jnp.logical_not(late)
@@ -409,13 +392,13 @@
         greet(2)
         greet(3)
 
-    take(0)
+    take(0, 0)
 
     @pl.when(soon)
     def _():
         greet(1)
 
-    take(1)
+    take(0, 1)
 
     @pl.when(soon)
     def _():
@@ -423,32 +406,31 @@
 
     local_copies[1].wait()
     inbox[st] = store_v[wanted_row(lambda pick, b: ids[pick, b])]
-    take(2)
+    take(0, 2)
 
     @pl.when(soon)
     def _():
         greet(3)
 
-    take(3)
+    take(0, 3)
     pl.when(late)(gather_all)
-    take(4)
+    take(0, 4)
     pl.when(late)(send_all)
-    take(5)
+    take(0, 5)
     pl.when(soon)(gather_all)
     for copy in local_copies[2:]:
         copy.wait()
     for chunk in range(RING):
         wg_f[chunk] = wg_v[:, chunk * 512 : (chunk + 1) * 512].astype(F32)
-    add_own_tokens(0)
-    take(6)
+    add_own(0)
+    take(0, 6)
     pl.when(soon)(send_all)
-    add_own_tokens(1)
-    add(0)
-    take(7)
-    add(1)
-    take(8)
-    add(2)
-    take(9)
+    add(0, 0, 1)
+    take(0, 7)
+    add(0, 2, 3)
+    take(0, 8)
+    add(0, 4, 5)
+    take(0, 9)
     for place in range(N_ST - 1):
         row_copy(place, source(place)).wait_recv()
     for b in range(BLOCKS):
@@ -456,14 +438,15 @@
             owner = lax.shift_right_logical(ids[pick, b], PASS_SHIFT)
             x[1, z, core, b, pick * PASS_ROWS : (pick + 1) * PASS_ROWS, :] = inbox[owner]
 
-    add(3)
+    add(0, 6)
     send_own(1)
-    take(10)
-    add(4)
-    take(11)
-    take(12)
-    add(5)
-    take(13)
+    add(0, 7)
+    take(0, 10)
+    take(0, 11)
+    take(0, 12)
+    add(0, 8, 9)
+    take(0, 13)
+    add(0, 10, 11)
 
     rate = decay[0]
 
@@ -505,52 +488,45 @@
         raw = acc_p[b, :, 0:128]
         mean = jnp.mean(raw * raw, axis=1, keepdims=True)
         pass_key = (raw * lax.rsqrt(mean + norm_eps)).astype(BF16)
-        pass_value = acc_p[b, :, 128:256].astype(BF16)
+        lifted = dot(acc_p[b, :, 128:256].astype(BF16), wl_v[0]).astype(BF16)
         exponent = jnp.exp(dot_t(mem_q[b], pass_key) * MEM_DIM ** (-0.5))
         mass = jnp.sum(exponent, axis=1, keepdims=True)
-        summed = dot(exponent.astype(BF16), pass_value)
-        mem_out = (summed / mass).astype(BF16)
-        lift = dot(mem_out, wl_v[0])
-        gate = gate_v[b]
+        gate = gate_v[b] / mass
         gate = jnp.concatenate([gate, gate], axis=1)
+        lift = dot(exponent.astype(BF16), lifted)
         out[b * BLOCK : (b + 1) * BLOCK, :] = (ret_norm[b] + gate * lift).astype(BF16)
 
+    def hand_done(phase):
+        hand_copy(phase, 0, -BLOCKS, core, BLOCKS).wait_send()
+        for d in range(2):
+            for first, count in hand_groups[phase]:
+                hand_copy(phase, d, first, core, count).wait_send()
+
     for step in range(SLOTS):
-        s = jnp.int32(step)
-        take_slot(1, s, step < SLOTS - BLOCKS)
-        if step >= SLOTS - 2:
-            hand_slot(1, s)
-        elif step % 2:
-            hand_pair(1, jnp.int32(step // 2))
+        take(1, step)
         if step == 0:
-            add(PAIRS - 1)
-            for pair in range(2):
-                own_copy(1, pair, other).wait_recv()
-                add_passages(z, 2 * pair, first=True)
-                add_passages(z, 2 * pair + 1, first=True)
-        elif step % 2 == 0:
-            add_pair(1, jnp.int32(step // 2 - 1))
-        if step < BLOCKS:
-            finish_tokens(step)
-        if step == 8:
+            add(0, 12, 13)
+            add_own(1)
+        if step % 2 == 0 and step > 0:
+            add(1, step - 2, step - 1)
+        if 1 <= step <= BLOCKS:
+            finish_tokens(step - 1)
+        if step == 9:
 
             @pl.loop(0, SLOTS)
             def _(n):
                 z_copy(0, 0, n).wait_send()
                 z_copy(0, 1, n).wait_send()
 
-            @pl.loop(0, 2 + 2 * PAIRS)
-            def _(n):
-                d_copy(0, n, z, 0, core).wait_send()
-
+            hand_done(0)
             for place in range(N_ST - 1):
                 id_copy(place, st).wait_send()
                 row_copy(place, st).wait_send()
 
-    add_slot(1, jnp.int32(SLOTS - 2))
+    add(1, 12)
     finish_block(0)
     finish_block(2)
-    add_slot(1, jnp.int32(SLOTS - 1))
+    add(1, 13)
     finish_block(1)
     finish_block(3)
 
@@ -559,14 +535,7 @@
         z_copy(1, 0, n).wait_send()
         z_copy(1, 1, n).wait_send()
 
-    for pair in range(2):
-        own_copy(1, pair, core).wait_send()
-    for pair in range(PAIRS - 1):
-        for d in range(2):
-            pair_copy(1, d, pair, core).wait_send()
-    for s in (SLOTS - 2, SLOTS - 1):
-        for d in range(2):
-            slot_copy(1, d, s, core).wait_send()
+    hand_done(1)
 
 
 def per_device(
@@ -633,8 +602,8 @@
             dma((12,)),
             dma((2, 2, SLOTS)),
             dma((2, 2, SLOTS)),
-            dma((2, 6 + 2 * PAIRS)),
-            dma((2, 6 + 2 * PAIRS)),
+            dma((2, 2, BLOCKS + SLOTS)),
+            dma((2, 2, BLOCKS + SLOTS)),
             dma((N_ST,)),
             dma((N_ST,)),
             dma((N_ST,)),

time: 55.5 us -> 55.1 us (level)
  no operation moved by 1% of the time
where the time goes in v6:
time: 55.1 us; the launch traced here: 55 us
  Pallas kernels  53.6 us (97%)
  local copies, waits for them, and re-layouts  0.71 us (1%)
  between operations  0.66 us (1%)
    pallas_call x1, Pallas kernels, per_device(): pl.pallas_call(kernel, out_shape=pltpu.VMEM((SEQ_LEN, VALUE_DIM), BF16),...  53.6 us

profile of v6, /device:TPU:1, one launch (start us, length us, event | category | flops | bytes accessed | tf_op | source)
XLA Modules:
  0.0 55.0 jit_solution(13186495003088855195)
XLA Ops:
  0.7 53.6 %fused_layer.1 = bf16[512,256]{1,0:T(8,128)(2,1)S(1)} custom-call(f32[1]{0:T(128)S(6)} %copy.17.decay, bf16[512,256]{1,0:T(8,128)(2,1)} %tok.1, bf16[4096,128]{1,0:T(8,128)(2,1)} %wq.1, bf16[4096,128]{1,0:T(8,128)(2,1)} %wk.1, bf16[4096,256]{1,0:T(8,128)(2,1)} %wv.1, bf16[4096,128]{1,0:T(8,128)(2,1)} %wmq.1, bf16[4096,128]{1,0:T(8,128)(2,1)} %wmk.1, ...), custom_call_target="tpu_custom_call" | custom-call | tf_op jit(solution)/shard_map/fused_layer/pallas_call | solution.py:573
  54.3 0.7 %copy.16 = bf16[512,256]{1,0:T(8,128)(2,1)} copy(bf16[512,256]{1,0:T(8,128)(2,1)S(1)} %fused_layer.1) | data formatting | bytes 524288

commit v7 on v6

--- a/solution.py
+++ b/solution.py
@@ -509,8 +509,8 @@
             add_own(1)
         if step % 2 == 0 and step > 0:
             add(1, step - 2, step - 1)
-        if 1 <= step <= BLOCKS:
-            finish_tokens(step - 1)
+        if step in (1, 3, 5, 7):
+            finish_tokens(step // 2)
         if step == 9:
 
             @pl.loop(0, SLOTS)

time: 55.1 us -> 55.1 us (level)
  no operation moved by 1% of the time
where the time goes in v7:
time: 55.1 us; the launch traced here: 55 us
  Pallas kernels  53.6 us (97%)
  local copies, waits for them, and re-layouts  0.71 us (1%)
  between operations  0.66 us (1%)
    pallas_call x1, Pallas kernels, per_device(): pl.pallas_call(kernel, out_shape=pltpu.VMEM((SEQ_LEN, VALUE_DIM), BF16),...  53.6 us

profile of v7, /device:TPU:1, one launch (start us, length us, event | category | flops | bytes accessed | tf_op | source)
XLA Modules:
  0.0 55.0 jit_solution(14229433543298861969)
XLA Ops:
  0.7 53.6 %fused_layer.1 = bf16[512,256]{1,0:T(8,128)(2,1)S(1)} custom-call(f32[1]{0:T(128)S(6)} %copy.17.decay, bf16[512,256]{1,0:T(8,128)(2,1)} %tok.1, bf16[4096,128]{1,0:T(8,128)(2,1)} %wq.1, bf16[4096,128]{1,0:T(8,128)(2,1)} %wk.1, bf16[4096,256]{1,0:T(8,128)(2,1)} %wv.1, bf16[4096,128]{1,0:T(8,128)(2,1)} %wmq.1, bf16[4096,128]{1,0:T(8,128)(2,1)} %wmk.1, ...), custom_call_target="tpu_custom_call" | custom-call | tf_op jit(solution)/shard_map/fused_layer/pallas_call | solution.py:573
  54.3 0.7 %copy.16 = bf16[512,256]{1,0:T(8,128)(2,1)} copy(bf16[512,256]{1,0:T(8,128)(2,1)S(1)} %fused_layer.1) | data formatting | bytes 524288
